TPU v7x, 256 devices: a whole 4x4x8 slice. The times are simulated.
256 devices in a mesh: sp: 16 (over y, x), tp: 16 (over z, core).
Axes of the slice: x: 4, y: 4, z: 8, core: 2. Of those that a mesh axis runs over, the one named last changes fastest.
Arguments:
- latent: bfloat16 [8192, 4096], P(('sp', 'tp')), may hold values from -6 to 6
- context: bfloat16 [512, 4096], P('sp'), may hold values from -6 to 6
- condition: float32 [4096], replicated, may hold values from -6 to 6
- context_condition: float32 [4096], replicated, may hold values from -6 to 6
- modulation: bfloat16 [3, 4096, 4096], P(None, 'sp', 'tp'), may hold values from -0.09375 to 0.09375
- query_weight: bfloat16 [4096, 4096], P(None, 'tp'), as said below
- key_weight: bfloat16 [4096, 4096], P(None, 'tp'), as said below
- value_weight: bfloat16 [4096, 4096], P(None, 'tp'), may hold values from -0.09375 to 0.09375
- lambdas: float32 [16], P('tp'), may hold values from 0.3 to 0.8
- context_lift: float32 [16], P('tp'), may hold values from 1.5 to 3
- head_gain: float32 [256], replicated, may hold values from 0.1 to 1.9
- output_weight: bfloat16 [4096, 4096], P('tp'), may hold values from -0.09375 to 0.09375
Outputs:
- result: bfloat16 [8192, 4096], P(('sp', 'tp'))
Inputs may be any that keep to these rules, and one draw needn't show every extreme that they name: `query_weight`: entries lie within 200 / sqrt(4096) in magnitude. `key_weight`: entries lie within 6 / sqrt(4096) in magnitude.
All inputs are finite; a program needn't handle non-finite values.
Results may differ from a plain program's by a relative error of at most 0.025.
Values may be sent and summed in bfloat16 or wider, within the bound.
A program may use at most 64 MiB of HBM per device.

v0:
```python
import functools

import jax
import jax.numpy as jnp
from jax import lax
from jax.experimental import pallas as pl
from jax.experimental.pallas import tpu as pltpu
from jax.sharding import PartitionSpec as P

GRID_W = 64
ROPE_BASE = 10000.0
EPSILON = 1e-05
LOG2E = 1.4426950408889634
ROWS = 16
VMEM_LIMIT = 62 * 1024 * 1024
MESH = pl.DeviceIdType.MESH


def remote(src, dst, send_sem, recv_sem, **where):
    return pltpu.make_async_remote_copy(
        src_ref=src,
        dst_ref=dst,
        send_sem=send_sem,
        recv_sem=recv_sem,
        device_id=where,
        device_id_type=MESH,
    )


def aligned(start, size, unit):
    return pl.ds(pl.multiple_of(start, unit), size)


def attend_kernel(
    sp_size,
    tp_size,
    latent,
    context,
    condition,
    context_condition,
    modulation,
    query_weight,
    key_weight,
    value_weight,
    cosine,
    sine,
    lambdas,
    lift,
    gain,
    attended,
    gate,
    tokens,
    context_tokens,
    normed,
    mod_weight,
    wq,
    wk,
    wv,
    keys_values,
    queries,
    kv_stage,
    q_stage,
    out_stage,
    mod_parts,
    mod_pieces,
    mod_rows,
    local_sem,
    tok_send,
    tok_recv,
    part_send,
    part_recv,
    piece_send,
    piece_recv,
    kv_send,
    kv_recv,
    q_send,
    q_recv,
    out_send,
    out_recv,
):
    s = lax.axis_index("sp")
    t = lax.axis_index("tp")
    z = lax.div(t, 2)
    c = lax.rem(t, 2)
    chips = tp_size // 2
    rows, width = latent.shape
    pair = 2 * rows
    block_tokens = tp_size * rows
    ctx_rows = context.shape[0]
    ctx_total = ctx_rows * sp_size
    local = query_weight.shape[1]
    heads = lambdas.shape[0]
    head = local // heads
    half = head // 2
    piece = modulation.shape[2]
    depth = modulation.shape[1]

    own_slot = tokens.at[aligned(t * rows, rows, ROWS)]
    locals_ = [
        pltpu.make_async_copy(src, dst, local_sem.at[i])
        for i, (src, dst) in enumerate(
            [
                (modulation, mod_weight),
                (latent, own_slot),
                (context, context_tokens),
                (key_weight, wk),
                (value_weight, wv),
                (query_weight, wq),
            ]
        )
    ]
    for copy in locals_:
        copy.start()

    barrier = pltpu.get_barrier_semaphore()
    for k in range(1, tp_size):
        pl.semaphore_signal(
            barrier, inc=1, device_id={"tp": lax.rem(t + k, tp_size)}, device_id_type=MESH
        )
    for k in range(1, sp_size):
        pl.semaphore_signal(
            barrier, inc=1, device_id={"sp": lax.rem(s + k, sp_size)}, device_id_type=MESH
        )
    pl.semaphore_wait(barrier, tp_size + sp_size - 2)

    part_rows = rows // 2

    def token_copy(kind, b, core, part, own=False):
        slot = 2 * b + core
        place = tokens.at[aligned(slot * rows + part * part_rows, part_rows, ROWS)]
        to = (t + 2, t - 2, t + 1 - 2 * c)[kind]
        return remote(
            latent.at[part * part_rows : (part + 1) * part_rows] if own else place,
            place,
            tok_send.at[kind, 2 * b + part],
            tok_recv.at[2 * slot + part],
            tp=to,
        )

    for part in range(2):

        @pl.when(z + 1 < chips)
        def _():
            token_copy(0, z, c, part, True).start()

        @pl.when(z > 0)
        def _():
            token_copy(1, z, c, part, True).start()

        token_copy(2, z, c, part, True).start()

    def silu(ref):
        v = ref[:, aligned(s * depth, depth, 128)]
        return v / (1.0 + jnp.exp(-v))

    first = silu(condition)
    second = silu(context_condition)
    which = lax.broadcasted_iota(jnp.int32, (ROWS, depth), 0)
    vectors = jnp.where(
        which == 0, jnp.broadcast_to(first, (ROWS, depth)), jnp.broadcast_to(second, (ROWS, depth))
    ).astype(jnp.bfloat16)
    locals_[0].wait()
    for r in range(3):
        found = jnp.dot(vectors, mod_weight[r], preferred_element_type=jnp.float32)
        mod_parts[s, 2 * r : 2 * r + 2, :] = found[0:2]
    mod_parts[s, 6:8, :] = jnp.zeros((2, piece), jnp.float32)

    def part_copy(k, owner):
        return remote(
            mod_parts.at[owner],
            mod_parts.at[owner],
            part_send.at[k],
            part_recv.at[owner],
            sp=lax.rem(s + k, sp_size),
        )

    def piece_copy(k, owner):
        return remote(
            mod_pieces.at[owner],
            mod_pieces.at[owner],
            piece_send.at[k],
            piece_recv.at[owner],
            tp=lax.rem(t + k, tp_size),
        )

    for k in range(1, sp_size):
        part_copy(k, s).start()
    for k in range(1, sp_size):
        part_copy(k, lax.rem(s + k, sp_size)).wait_recv()
    total = mod_parts[0]
    for i in range(1, sp_size):
        total = total + mod_parts[i]
    mod_pieces[t] = total
    for k in range(1, tp_size):
        piece_copy(k, t).start()

    def forward(d):
        left = z - d
        right = z + d

        for part in range(2):

            @pl.when(left >= 0)
            def _():
                token_copy(2, left, c, part).wait_recv()

                @pl.when(z + 1 < chips)
                def _():
                    token_copy(0, left, c, part).start()

                token_copy(2, left, c, part).start()

            @pl.when(right < chips)
            def _():
                token_copy(2, right, c, part).wait_recv()

                @pl.when(z > 0)
                def _():
                    token_copy(1, right, c, part).start()

                token_copy(2, right, c, part).start()

    forward(1)
    for k in range(1, tp_size):
        piece_copy(k, lax.rem(t + k, tp_size)).wait_recv()
    for i in range(tp_size):
        mod_rows[:, i * piece : (i + 1) * piece] = mod_pieces[i]
    gate[...] = mod_rows[4:5, :]

    def normalise(source, base, count, row):
        def group(i, carry):
            x = source[aligned(base + i * ROWS, ROWS, ROWS), :].astype(jnp.float32)
            x = x - jnp.sum(x, axis=1, keepdims=True) * (1.0 / width)
            spread = jnp.sum(x * x, axis=1, keepdims=True) * (1.0 / width)
            y = x * lax.rsqrt(spread + EPSILON)
            y = y * (1.0 + mod_rows[2 + row : 3 + row, :]) + mod_rows[row : row + 1, :]
            normed[aligned(i * ROWS, ROWS, ROWS), :] = y.astype(jnp.bfloat16)
            return carry

        lax.fori_loop(0, count // ROWS, group, 0)

    my_head = lax.rem(s, heads)

    def mate(k):
        return lax.rem(my_head + k, heads)

    def kv_place(owner, b, is_context):
        if is_context:
            return aligned(owner * ctx_rows, ctx_rows, ROWS)
        return aligned(ctx_total + owner * block_tokens + b * pair, pair, ROWS)

    def stage_place(b, is_context):
        if is_context:
            return aligned(block_tokens, ctx_rows, ROWS)
        return aligned(b * pair, pair, ROWS)

    def kv_copy(k, owner, b, is_context):
        to = lax.rem(s + k, sp_size)
        return remote(
            kv_stage.at[lax.rem(to, heads), stage_place(b, is_context)],
            keys_values.at[kv_place(owner, b, is_context)],
            kv_send.at[k, b],
            kv_recv.at[owner, b],
            sp=to,
        )

    def q_copy(k, slot, b):
        place = aligned(b * pair, pair, ROWS)
        return remote(
            q_stage.at[mate(k), place],
            queries.at[slot, place],
            q_send.at[k, b],
            q_recv.at[slot, b],
            sp=s - my_head + mate(k),
        )

    def out_copy(k, head_index):
        return remote(
            out_stage.at[mate(k)],
            attended.at[head_index],
            out_send.at[k],
            out_recv.at[head_index],
            sp=s - my_head + mate(k),
        )

    def hand_out(keys, values, b, is_context):
        place = stage_place(b, is_context)
        for g in range(heads):
            kv_stage[g, place, :head] = keys[:, g * head : (g + 1) * head]
            kv_stage[g, place, head:] = values[:, g * head : (g + 1) * head]
        for k in range(1, sp_size):
            kv_copy(k, s, b, is_context).start()
        keys_values[kv_place(s, b, is_context), :] = kv_stage[my_head, place, :]

    locals_[1].wait()
    for i in (3, 4, 5):
        locals_[i].wait()

    quarter = half // 4
    lane = lax.broadcasted_iota(jnp.int32, (pair, half), 1)
    low = lax.rem(lane, 2 * quarter) < quarter

    def turn(raw, b):
        cos = cosine[aligned(b * pair, pair, ROWS), :]
        sin = sine[aligned(b * pair, pair, ROWS), :]
        parts = []
        for i in range(local // half):
            v = raw[:, i * half : (i + 1) * half].astype(jnp.bfloat16).astype(jnp.float32)
            other = jnp.where(low, pltpu.roll(v, half - quarter, 1), pltpu.roll(v, quarter, 1))
            parts.append((v * cos + other * sin).astype(jnp.bfloat16))
        return jnp.concatenate(parts, axis=1)

    def process(b):
        for part in range(2):
            token_copy(2, b, 1 - c, part).wait_recv()
        normalise(tokens, b * pair, pair, 0)
        x = normed[:pair, :]
        hand_out(
            turn(jnp.dot(x, wk[...], preferred_element_type=jnp.float32), b),
            jnp.dot(x, wv[...], preferred_element_type=jnp.float32).astype(jnp.bfloat16),
            b,
            False,
        )
        turned = turn(jnp.dot(x, wq[...], preferred_element_type=jnp.float32), b)
        place = aligned(b * pair, pair, ROWS)
        for g in range(heads):
            q_stage[g, place, :] = turned[:, g * head : (g + 1) * head]
        for k in range(1, heads):
            q_copy(k, my_head, b).start()
        queries[my_head, place, :] = q_stage[my_head, place, :]

    def process_context():
        locals_[2].wait()
        normalise(context_tokens, 0, ctx_rows, 1)
        hand_out(
            jnp.dot(normed[:ctx_rows, :], wk[...], preferred_element_type=jnp.float32).astype(
                jnp.bfloat16
            ),
            jnp.dot(normed[:ctx_rows, :], wv[...], preferred_element_type=jnp.float32).astype(
                jnp.bfloat16
            ),
            chips,
            True,
        )

    def step(j, carry):
        d = lax.div(j, 2)
        side = lax.rem(j, 2)

        @pl.when(j == 1)
        def _():
            if chips > 2:
                forward(2)
            process_context()

        @pl.when((side == 0) & (d >= 2) & (d + 1 < chips))
        def _():
            forward(d + 1)

        b = z - d + 2 * d * side

        @pl.when((b >= 0) & (b < chips) & (d + 1 > side))
        def _():
            process(b)

        return carry

    lax.fori_loop(0, 2 * chips, step, 0)

    for k in range(1, sp_size):
        owner = lax.rem(s + k, sp_size)
        kv_copy(k, owner, chips, True).wait_recv()
        for b in range(chips):
            kv_copy(k, owner, b, False).wait_recv()
    for k in range(1, heads):
        for b in range(chips):
            q_copy(k, mate(k), b).wait_recv()

    tile = min(256, block_tokens)
    key_total = keys_values.shape[0]
    factor = half ** (-0.5) * LOG2E
    on_context = lax.broadcasted_iota(jnp.int32, (1, key_total), 1) < ctx_total

    raised = jnp.where(on_context, lift[my_head] * LOG2E, 0.0)
    weight_of_second = lambdas[my_head]

    def attention(i, slot):
        place = aligned(i * tile, tile, ROWS)
        outs = []
        for m in range(2):
            scores = lax.dot_general(
                queries[slot, place, m * half : (m + 1) * half],
                keys_values[:, m * half : (m + 1) * half],
                (((1,), (1,)), ((), ())),
                preferred_element_type=jnp.float32,
            )
            scores = scores * factor + raised
            weights = jnp.exp2(scores - jnp.max(scores, axis=1, keepdims=True))
            sums = jnp.sum(weights, axis=1, keepdims=True)
            outs.append(
                jnp.dot(
                    weights.astype(jnp.bfloat16),
                    keys_values[:, head:],
                    preferred_element_type=jnp.float32,
                )
                / sums
            )
        diff = outs[0] - weight_of_second * outs[1]
        mean = jnp.sum(diff * diff, axis=1, keepdims=True) * (1.0 / head)
        out_stage[slot, place, :] = (diff * lax.rsqrt(mean + EPSILON) * gain[...]).astype(
            jnp.bfloat16
        )
        return slot

    for k in range(1, heads + 1):
        lax.fori_loop(0, block_tokens // tile, attention, mate(k))
        if k < heads:
            out_copy(k, my_head).start()
    attended[my_head] = out_stage[my_head]
    for k in range(1, heads):
        out_copy(k, mate(k)).wait_recv()
        out_copy(k, my_head).wait_send()
        for b in range(chips):
            q_copy(k, my_head, b).wait_send()

    for b in range(chips):
        for part in range(2):

            @pl.when((b <= z) & (z + 1 < chips))
            def _():
                token_copy(0, b, c, part).wait_send()

            @pl.when((b >= z) & (z > 0))
            def _():
                token_copy(1, b, c, part).wait_send()

            token_copy(2, b, c, part).wait_send()
    for k in range(1, tp_size):
        piece_copy(k, t).wait_send()
    for k in range(1, sp_size):
        part_copy(k, s).wait_send()
        kv_copy(k, s, chips, True).wait_send()
        for b in range(chips):
            kv_copy(k, s, b, False).wait_send()


def output_kernel(
    tp_size,
    attended,
    output_weight,
    latent,
    gate,
    result,
    weight,
    own,
    pair_send,
    pair_recv,
    stage,
    from_left,
    from_right,
    local_sem,
    ps_sem,
    pr_sem,
    st_sem,
    left_sem,
    right_sem,
):
    t = lax.axis_index("tp")
    z = lax.div(t, 2)
    c = lax.rem(t, 2)
    chips = tp_size // 2
    rows, width = latent.shape
    span = width // 2
    chunk = min(1024, span)

    load = pltpu.make_async_copy(output_weight, weight, local_sem)
    load.start()
    barrier = pltpu.get_barrier_semaphore()

    @pl.when(z > 0)
    def _():
        pl.semaphore_signal(barrier, inc=1, device_id={"tp": t - 2}, device_id_type=MESH)

    @pl.when(z + 1 < chips)
    def _():
        pl.semaphore_signal(barrier, inc=1, device_id={"tp": t + 2}, device_id_type=MESH)

    pl.semaphore_signal(barrier, inc=1, device_id={"tp": t + 1 - 2 * c}, device_id_type=MESH)
    inner = (z > 0) & (z + 1 < chips)
    pl.semaphore_wait(barrier, jnp.where(inner, 3, 2) if chips > 1 else 1)

    load.wait()

    def pair_copy(b):
        return remote(
            pair_send.at[b], pair_recv.at[b], ps_sem.at[b], pr_sem.at[b], tp=t + 1 - 2 * c
        )

    def right_copy(b):
        return remote(stage.at[b], from_left.at[b], st_sem.at[b], left_sem.at[b], tp=t + 2)

    def left_copy(b):
        return remote(stage.at[b], from_right.at[b], st_sem.at[b], right_sem.at[b], tp=t - 2)

    def compute(b, part):
        u = 2 * b + part
        other = aligned((2 * b + 1 - c) * rows, rows, ROWS)
        mine = aligned((2 * b + c) * rows, rows, ROWS)
        both = jnp.concatenate(
            [
                jnp.concatenate([attended[g, part, :] for g in range(attended.shape[0])], axis=1)
                for part in (other, mine)
            ],
            axis=0,
        )
        for n in range(span // chunk):
            cols = slice(n * chunk, (n + 1) * chunk)
            found = jnp.dot(
                both,
                weight[:, aligned(part * span + n * chunk, chunk, 128)],
                preferred_element_type=jnp.float32,
            )
            pair_send[u, :, cols] = found[:rows].astype(jnp.bfloat16)
            own[u, :, cols] = found[rows:]
        pair_copy(u).start()

    def combine(b, part):
        u = 2 * b + part
        pair_copy(u).wait_recv()

        @pl.when(b > z)
        def _():
            @pl.when(z > 0)
            def _():
                right_copy(u).wait_recv()
                stage[u] = (
                    own[u] + pair_recv[u].astype(jnp.float32) + from_left[u].astype(jnp.float32)
                ).astype(jnp.bfloat16)

            @pl.when(z == 0)
            def _():
                stage[u] = (own[u] + pair_recv[u].astype(jnp.float32)).astype(jnp.bfloat16)

            right_copy(u).start()

        @pl.when(b < z)
        def _():
            @pl.when(z + 1 < chips)
            def _():
                left_copy(u).wait_recv()
                stage[u] = (
                    own[u] + pair_recv[u].astype(jnp.float32) + from_right[u].astype(jnp.float32)
                ).astype(jnp.bfloat16)

            @pl.when(z + 1 == chips)
            def _():
                stage[u] = (own[u] + pair_recv[u].astype(jnp.float32)).astype(jnp.bfloat16)

            left_copy(u).start()

    def place_of(j):
        d = chips - 1 - lax.div(j, 4)
        side = lax.rem(lax.div(j, 2), 2)
        b = z - d + 2 * d * side
        return b, lax.rem(j, 2), (b >= 0) & (b < chips) & (d + 1 > side)

    at_end = (z == 0) | (z + 1 == chips)

    def first_pass(j, carry):
        b, part, valid = place_of(j)

        @pl.when(valid)
        def _():
            compute(b, part)

            @pl.when(at_end & (b != z))
            def _():
                combine(b, part)

        return carry

    lax.fori_loop(0, 4 * chips, first_pass, 0)

    def second_pass(j, carry):
        b, part, valid = place_of(j)

        @pl.when(valid & jnp.logical_not(at_end) & (b != z))
        def _():
            combine(b, part)

        return carry

    lax.fori_loop(0, 4 * chips, second_pass, 0)

    for part in range(2):
        u = 2 * z + part
        cols = slice(part * span, (part + 1) * span)
        pair_copy(u).wait_recv()
        own[u] = own[u] + pair_recv[u].astype(jnp.float32)

        @pl.when(z > 0)
        def _():
            right_copy(u).wait_recv()
            own[u] = own[u] + from_left[u].astype(jnp.float32)

        @pl.when(z + 1 < chips)
        def _():
            left_copy(u).wait_recv()
            own[u] = own[u] + from_right[u].astype(jnp.float32)

        result[:, cols] = (latent[:, cols].astype(jnp.float32) + gate[:, cols] * own[u]).astype(
            jnp.bfloat16
        )

    for u in range(2 * chips):
        pair_copy(u).wait_send()

        @pl.when(u // 2 > z)
        def _():
            right_copy(u).wait_send()

        @pl.when(u // 2 < z)
        def _():
            left_copy(u).wait_send()


def tables(places, half):
    quarter = half // 4
    inverse = ROPE_BASE ** (-jnp.arange(quarter, dtype=jnp.float32) / quarter)
    by_row = (places // GRID_W).astype(jnp.float32)[:, None] * inverse
    by_col = (places % GRID_W).astype(jnp.float32)[:, None] * inverse
    angles = jnp.concatenate([by_row, by_row, by_col, by_col], axis=1)
    sign = jnp.where(jnp.arange(half) % (2 * quarter) < quarter, -1.0, 1.0)
    return jnp.cos(angles), jnp.sin(angles) * sign


def shards(
    sp_size,
    tp_size,
    latent,
    context,
    condition,
    context_condition,
    modulation,
    query_weight,
    key_weight,
    value_weight,
    lambdas,
    context_lift,
    head_gain,
    output_weight,
):
    rows, width = latent.shape
    chips = tp_size // 2
    local = query_weight.shape[1]
    heads = lambdas.shape[0]
    head = local // heads
    half = head // 2
    block_tokens = rows * tp_size
    ctx_rows = context.shape[0]
    piece = modulation.shape[2]
    places = lax.axis_index("sp") * block_tokens + jnp.arange(block_tokens, dtype=jnp.int32)
    cosine, sine = tables(places, half)
    vmem = pl.BlockSpec(memory_space=pltpu.VMEM)
    smem = pl.BlockSpec(memory_space=pltpu.SMEM)
    anywhere = pl.BlockSpec(memory_space=pl.ANY)
    bf16, f32 = jnp.bfloat16, jnp.float32
    dma = pltpu.SemaphoreType.DMA
    attended, gate = pl.pallas_call(
        functools.partial(attend_kernel, sp_size, tp_size),
        out_shape=(
            jax.ShapeDtypeStruct((heads, block_tokens, head), bf16),
            jax.ShapeDtypeStruct((1, width), f32),
        ),
        in_specs=[anywhere] * 2 + [vmem] * 2 + [anywhere] * 4 + [vmem] * 2 + [smem] * 2 + [vmem],
        out_specs=(vmem, vmem),
        scratch_shapes=[
            pltpu.VMEM((block_tokens, width), bf16),
            pltpu.VMEM(context.shape, bf16),
            pltpu.VMEM((max(2 * rows, ctx_rows), width), bf16),
            pltpu.VMEM(modulation.shape, bf16),
            pltpu.VMEM((width, local), bf16),
            pltpu.VMEM((width, local), bf16),
            pltpu.VMEM((width, local), bf16),
            pltpu.VMEM((sp_size * (ctx_rows + block_tokens), 2 * head), bf16),
            pltpu.VMEM((heads, block_tokens, head), bf16),
            pltpu.VMEM((heads, block_tokens + ctx_rows, 2 * head), bf16),
            pltpu.VMEM((heads, block_tokens, head), bf16),
            pltpu.VMEM((heads, block_tokens, head), bf16),
            pltpu.VMEM((sp_size, 8, piece), f32),
            pltpu.VMEM((tp_size, 8, piece), f32),
            pltpu.VMEM((8, width), f32),
            dma((6,)),
            dma((3, 2 * chips)),
            dma((2 * tp_size,)),
            dma((sp_size,)),
            dma((sp_size,)),
            dma((tp_size,)),
            dma((tp_size,)),
            dma((sp_size, chips + 1)),
            dma((sp_size, chips + 1)),
            dma((heads, chips)),
            dma((heads, chips)),
            dma((heads,)),
            dma((heads,)),
        ],
        compiler_params=pltpu.CompilerParams(
            collective_id=0, has_side_effects=True, vmem_limit_bytes=VMEM_LIMIT
        ),
        name="attend",
    )(
        latent,
        context,
        condition.reshape(1, -1),
        context_condition.reshape(1, -1),
        modulation,
        query_weight,
        key_weight,
        value_weight,
        cosine,
        sine,
        lambdas,
        context_lift,
        head_gain.reshape(1, -1),
    )
    blocks = (2 * chips, rows, width // 2)
    return pl.pallas_call(
        functools.partial(output_kernel, tp_size),
        out_shape=jax.ShapeDtypeStruct((rows, width), bf16),
        in_specs=[vmem, anywhere, vmem, vmem],
        out_specs=vmem,
        scratch_shapes=[
            pltpu.VMEM(output_weight.shape, bf16),
            pltpu.VMEM(blocks, f32),
            pltpu.VMEM(blocks, bf16),
            pltpu.VMEM(blocks, bf16),
            pltpu.VMEM(blocks, bf16),
            pltpu.VMEM(blocks, bf16),
            pltpu.VMEM(blocks, bf16),
            dma(()),
            dma((2 * chips,)),
            dma((2 * chips,)),
            dma((2 * chips,)),
            dma((2 * chips,)),
            dma((2 * chips,)),
        ],
        compiler_params=pltpu.CompilerParams(
            collective_id=1, has_side_effects=True, vmem_limit_bytes=VMEM_LIMIT
        ),
        name="output",
    )(attended, output_weight, latent, gate)


def solution(mesh):
    in_specs = (
        P(("sp", "tp"), None),
        P("sp", None),
        P(),
        P(),
        P(None, "sp", "tp"),
        P(None, "tp"),
        P(None, "tp"),
        P(None, "tp"),
        P("tp"),
        P("tp"),
        P(),
        P("tp", None),
    )
    out_specs = P(("sp", "tp"), None)
    body = functools.partial(shards, mesh.shape["sp"], mesh.shape["tp"])
    return jax.shard_map(body, mesh=mesh, in_specs=in_specs, out_specs=out_specs, check_vma=False)
```

profile of v0, /device:TPU:1, one launch (start us, length us, event | category | flops | bytes accessed | tf_op | source)
XLA Modules:
  0.0 201.8 jit_solution(9468576613873280929)
XLA Ops:
  0.0 0.2 broadcast_multiply_fusion.1
  0.2 1.9 sine_multiply_fusion
  3.4 150.8 %attend.1 = (bf16[1,512,256]{2,1,0:T(8,128)(2,1)}, f32[1,4096]{1,0:T(1,128)}) custom-call(bf16[32,4096]{1,0:T(8,128)(2,1)} %latent.3, bf16[32,4096]{1,0:T(8,128)(2,1)} %context.1, f32[1,4096]{1,0:T(1,128)} %bitcast.3, f32[1,4096]{1,0:T(1,128)} %bitcast.4, bf16[3,256,256]{2,1,0:T(8,128)(2,1)} %modulation.1, bf16[4096,256]{1,0:T(8,128)(2,1)} %query_weight.1, ...), custom_call_target="tpu_custom_call" | custom-call | tf_op jit(solution)/shard_map/attend/pallas_call | solution.py:669
  154.2 45.9 %output.1 = bf16[32,4096]{1,0:T(8,128)(2,1)} custom-call(bf16[1,512,256]{2,1,0:T(8,128)(2,1)} %get-tuple-element.7.attended, bf16[256,4096]{1,0:T(8,128)(2,1)} %output_weight.1, bf16[32,4096]{1,0:T(8,128)(2,1)} %latent.3, f32[1,4096]{1,0:T(1,128)} %get-tuple-element.8.gate), custom_call_target="tpu_custom_call" | custom-call | tf_op jit(solution)/shard_map/output/pallas_call | solution.py:727
  200.1 1.7 copy.16
  (3 shorter events, 0.0 us)
where the time goes:
time: 202 us
  Pallas kernels  197 us (98%)
  other arithmetic  2.09 us (1%)
    pallas_call x1, Pallas kernels, shards(): pl.pallas_call(functools.partial(attend_kernel, sp_size, tp_size), out_sh...  151 us
    pallas_call x1, Pallas kernels, shards(): pl.pallas_call(functools.partial(output_kernel, tp_size), out_shape=jax.S...  45.9 us

commit v1 on v0

v1 whole, which is shorter than its diff:
```python
import functools

import jax
import jax.numpy as jnp
import numpy as np
from jax import lax
from jax.experimental import pallas as pl
from jax.experimental.pallas import tpu as pltpu
from jax.sharding import PartitionSpec as P

GRID_W = 64
ROPE_BASE = 10000.0
EPSILON = 1e-05
LOG2E = 1.4426950408889634
ROWS = 16
SIDE = 4
VMEM_LIMIT = 63 * 1024 * 1024
MESH = pl.DeviceIdType.MESH
ROW_FIRST = (1, 3, 4)
COLUMN_FIRST = (0, 2)


def aligned(start, size, unit=ROWS):
    return pl.ds(pl.multiple_of(start, unit), size)


def kernel(
    sp_size,
    tp_size,
    latent,
    context,
    condition,
    context_condition,
    modulation,
    query_weight,
    key_weight,
    value_weight,
    row_cos,
    row_sin,
    col_cos,
    col_sin,
    lambdas,
    lift,
    gain,
    output_weight,
    result,
    tokens,
    context_tokens,
    normed,
    mod_weight,
    wq,
    wk,
    wv,
    wo,
    keys_values,
    transit,
    stage,
    queries,
    q_stage,
    peak,
    total_weight,
    mixed,
    attended,
    out_stage,
    mod_parts,
    mod_pieces,
    mod_rows,
    own,
    pair_send,
    pair_recv,
    ring_stage,
    from_left,
    from_right,
    local_sem,
    tok_send,
    tok_recv,
    part_send,
    part_recv,
    piece_send,
    piece_recv,
    kv_send,
    row_recv,
    y_recv,
    y2_recv,
    col_recv,
    x_recv,
    dd_own,
    dd_ownb,
    dd_all,
    q_send,
    q_recv,
    out_send,
    out_recv,
    ps_sem,
    pr_sem,
    st_sem,
    left_sem,
    right_sem,
):
    s = lax.axis_index("sp")
    t = lax.axis_index("tp")
    y = lax.div(s, SIDE)
    x = lax.rem(s, SIDE)
    z = lax.div(t, 2)
    c = lax.rem(t, 2)
    p = lax.rem(x, 2)
    chips = tp_size // 2
    far = chips // 2
    rows, width = latent.shape
    pair = 2 * rows
    block_tokens = tp_size * rows
    ctx_rows = context.shape[0]
    head = query_weight.shape[1]
    half = head // 2
    piece = modulation.shape[2]
    depth = modulation.shape[1]

    def ring(v, n):
        return lax.rem(v + n, n)

    def remote(src, dst, send_sem, recv_sem, sx, sy, sz, sc):
        return pltpu.make_async_remote_copy(
            src_ref=src,
            dst_ref=dst,
            send_sem=send_sem,
            recv_sem=recv_sem,
            device_id={"sp": sy * SIDE + sx, "tp": 2 * sz + sc},
            device_id_type=MESH,
        )

    own_slot = tokens.at[aligned(t * rows, rows)]
    locals_ = [
        pltpu.make_async_copy(src, dst, local_sem.at[i])
        for i, (src, dst) in enumerate(
            [
                (modulation, mod_weight),
                (latent, own_slot),
                (context, context_tokens),
                (key_weight, wk),
                (value_weight, wv),
                (query_weight, wq),
                (output_weight, wo),
            ]
        )
    ]
    for copy in locals_:
        copy.start()

    barrier = pltpu.get_barrier_semaphore()
    for k in range(1, tp_size):
        pl.semaphore_signal(
            barrier, inc=1, device_id={"sp": s, "tp": lax.rem(t + k, tp_size)}, device_id_type=MESH
        )
    for k in range(1, sp_size):
        pl.semaphore_signal(
            barrier, inc=1, device_id={"sp": lax.rem(s + k, sp_size), "tp": t}, device_id_type=MESH
        )
    near = [(1, 0), (2, 0), (3, 0), (0, 1), (0, 3)]
    for dx, dy in near:
        pl.semaphore_signal(
            barrier,
            inc=1,
            device_id={
                "sp": lax.rem(y + dy, SIDE) * SIDE + lax.rem(x + dx, SIDE),
                "tp": 2 * z + 1 - c,
            },
            device_id_type=MESH,
        )

    def silu(ref):
        v = ref[:, aligned(s * depth, depth, 128)]
        return v / (1.0 + jnp.exp(-v))

    first = silu(condition)
    second = silu(context_condition)
    which = lax.broadcasted_iota(jnp.int32, (ROWS, depth), 0)
    vectors = jnp.where(
        which == 0, jnp.broadcast_to(first, (ROWS, depth)), jnp.broadcast_to(second, (ROWS, depth))
    ).astype(jnp.bfloat16)
    locals_[0].wait()
    for r in range(3):
        found = jnp.dot(vectors, mod_weight[r], preferred_element_type=jnp.float32)
        mod_parts[s, 2 * r : 2 * r + 2, :] = found[0:2]
    mod_parts[s, 6:8, :] = jnp.zeros((2, piece), jnp.float32)
    locals_[1].wait()

    pl.semaphore_wait(barrier, tp_size + sp_size - 2 + len(near))

    part_rows = rows // 2

    def token_copy(kind, b, core, part):
        slot = 2 * b + core
        place = tokens.at[aligned(slot * rows + part * part_rows, part_rows)]
        to_z = (ring(z + 1, chips), ring(z - 1, chips), z)[kind]
        return remote(
            place,
            place,
            tok_send.at[kind, 2 * b + part],
            tok_recv.at[2 * slot + part],
            x,
            y,
            to_z,
            1 - c if kind == 2 else c,
        )

    def part_copy(k, owner):
        return pltpu.make_async_remote_copy(
            src_ref=mod_parts.at[owner],
            dst_ref=mod_parts.at[owner],
            send_sem=part_send.at[k],
            recv_sem=part_recv.at[owner],
            device_id={"sp": lax.rem(s + k, sp_size), "tp": t},
            device_id_type=MESH,
        )

    def piece_copy(k, owner):
        return pltpu.make_async_remote_copy(
            src_ref=mod_pieces.at[owner],
            dst_ref=mod_pieces.at[owner],
            send_sem=piece_send.at[k],
            recv_sem=piece_recv.at[owner],
            device_id={"sp": s, "tp": lax.rem(t + k, tp_size)},
            device_id_type=MESH,
        )

    for k in range(1, sp_size):
        part_copy(k, s).start()
    for part in range(2):
        token_copy(0, z, c, part).start()
        token_copy(1, z, c, 1 - part).start()
        token_copy(2, z, c, part).start()

    for k in range(1, sp_size):
        part_copy(k, lax.rem(s + k, sp_size)).wait_recv()
    total = mod_parts[0]
    for i in range(1, sp_size):
        total = total + mod_parts[i]
    mod_pieces[t] = total
    mod_pieces[t, 6:7, :] = jnp.full((1, piece), lambdas[0], jnp.float32)
    mod_pieces[t, 7:8, :] = jnp.full((1, piece), lift[0], jnp.float32)
    for k in range(1, tp_size):
        piece_copy(k, t).start()

    def forward(d, early):
        left = ring(z - d, chips)
        right = ring(z + d, chips)
        right_part, left_part = (0, 1) if early else (1, 0)
        token_copy(2, left, c, right_part).wait_recv()
        if d + 1 < far or (d + 1 == far and early):
            token_copy(0, left, c, right_part).start()
        token_copy(2, left, c, right_part).start()
        token_copy(2, right, c, left_part).wait_recv()
        if d + 1 < far or (d + 1 == far and early):
            token_copy(1, right, c, left_part).start()
        token_copy(2, right, c, left_part).start()

    forward(1, True)
    forward(1, False)
    for k in range(1, tp_size):
        piece_copy(k, lax.rem(t + k, tp_size)).wait_recv()
    for i in range(tp_size):
        mod_rows[:, i * piece : (i + 1) * piece] = mod_pieces[i]

    def normalise(source, base, dest, count, row):
        def group(i, carry):
            v = source[aligned(base + i * ROWS, ROWS), :].astype(jnp.float32)
            v = v - jnp.sum(v, axis=1, keepdims=True) * (1.0 / width)
            spread = jnp.sum(v * v, axis=1, keepdims=True) * (1.0 / width)
            v = v * lax.rsqrt(spread + EPSILON)
            v = v * (1.0 + mod_rows[2 + row : 3 + row, :]) + mod_rows[row : row + 1, :]
            normed[aligned(dest + i * ROWS, ROWS), :] = v.astype(jnp.bfloat16)
            return carry

        lax.fori_loop(0, count // ROWS, group, 0)

    sizes = (ctx_rows + pair, 2 * pair, 2 * pair, 2 * pair, pair)
    starts = tuple(sum(sizes[:g]) for g in range(5))
    q_starts = (0, pair, 3 * pair, 5 * pair, 7 * pair)
    transit_starts = {0: 0, 2: SIDE * sizes[0]}
    halves = tuple(n // 2 for n in sizes)
    own_kind = p == c
    other_kind = p != c
    xs = [x, lax.rem(x + 1, SIDE), lax.rem(x + 2, SIDE), lax.rem(x + 3, SIDE)]
    ys = [y, lax.rem(y + 1, SIDE), lax.rem(y + 2, SIDE), lax.rem(y + 3, SIDE)]

    def kv_at(g, q, sx, sy, count=1):
        order = sy * SIDE + sx if g in ROW_FIRST else sx * SIDE + sy
        n = halves[g]
        return keys_values.at[aligned(sp_size * starts[g] + (q * sp_size + order) * n, count * n)]

    def transit_at(g, q, sy, count=1):
        n = halves[g]
        return transit.at[aligned(transit_starts[g] + (q * SIDE + sy) * n, count * n)]

    def stage_at(g, q):
        return stage.at[aligned(starts[g] + q * halves[g], halves[g])]

    def send(g, k, src, dst, recv_sem, sx, sy, sc):
        return remote(src, dst, kv_send.at[g, k], recv_sem, sx, sy, z, sc)

    def to_partner(g, k, ref, recv_sem=None):
        return send(g, k, ref, ref, dd_all.at[g] if recv_sem is None else recv_sem, x, y, 1 - c)

    def arrived(ref, recv_sem):
        remote(ref, ref, kv_send.at[0, 0], recv_sem, x, y, z, 1 - c).wait_recv()

    def leaving(g, step):
        mine = []
        add = mine.append
        if g in ROW_FIRST:
            i = ROW_FIRST.index(g)
            if step == 1:
                for q in range(2):
                    there = kv_at(g, q, x, y)
                    add((other_kind, send(g, q, stage_at(g, q), there, row_recv.at[i, 2], xs[1], y, q)))
                    add((other_kind, send(g, 2 + q, stage_at(g, q), there, row_recv.at[i, 0], xs[3], y, q)))
                    add((own_kind, send(g, 4 + q, stage_at(g, q), there, row_recv.at[i, 1], xs[2], y, q)))
                add((own_kind, send(g, 6, stage_at(g, 1 - c), kv_at(g, 1 - c, x, y), dd_own.at[g], x, y, 1 - c)))
                add((own_kind, send(g, 7, stage_at(g, c), kv_at(g, c, x, y), dd_ownb.at[g], x, y, 1 - c)))
            if step == 2:
                line = kv_at(g, c, 0, y, SIDE)
                add((None, send(g, 11, line, line, y_recv.at[i, 0], x, ys[1], c)))
                add((None, send(g, 12, line, line, y_recv.at[i, 1], x, ys[3], c)))
                for k in range(3):
                    add((None, to_partner(g, 8 + k, kv_at(g, c, xs[k + 1], y))))
            if step == 3:
                low = kv_at(g, c, 0, ys[3], 2)
                high = kv_at(g, c, 2, ys[1], 2)
                add((None, send(g, 15, low, low, y2_recv.at[i, 0], x, ys[1], c)))
                add((None, send(g, 16, high, high, y2_recv.at[i, 1], x, ys[3], c)))
                add((None, to_partner(g, 13, kv_at(g, c, 0, ys[3], SIDE))))
                add((None, to_partner(g, 14, kv_at(g, c, 0, ys[1], SIDE))))
            if step == 4:
                add((None, to_partner(g, 17, kv_at(g, c, 0, ys[2], SIDE))))
            return mine
        i = COLUMN_FIRST.index(g)
        if step == 1:
            for q in range(2):
                for kind, cond, there in ((0, own_kind, kv_at(g, q, x, y)), (1, other_kind, transit_at(g, q, y))):
                    add((cond, send(g, q, stage_at(g, q), there, col_recv.at[i, 3 * kind], x, ys[1], q)))
                    add((cond, send(g, 2 + q, stage_at(g, q), there, col_recv.at[i, 3 * kind + 1], x, ys[3], q)))
            add((own_kind, send(g, 6, stage_at(g, 1 - c), kv_at(g, 1 - c, x, y), dd_own.at[g], x, y, 1 - c)))
            add((other_kind, send(g, 6, stage_at(g, 1 - c), transit_at(g, 1 - c, y), dd_own.at[g], x, y, 1 - c)))
            add((own_kind, send(g, 7, stage_at(g, c), kv_at(g, c, x, y), dd_ownb.at[g], x, y, 1 - c)))
        if step == 2:
            below = kv_at(g, c, x, ys[3])
            above = transit_at(g, c, ys[1])
            add((None, send(g, 9, below, below, col_recv.at[i, 2], x, ys[1], c)))
            add((None, send(g, 11, above, above, col_recv.at[i, 5], x, ys[3], c)))
            add((None, to_partner(g, 8, below)))
            add((None, to_partner(g, 10, kv_at(g, c, x, ys[1]))))
        if step == 3:
            line = kv_at(g, c, x, 0, SIDE)
            passing = transit_at(g, c, 0, SIDE)
            add((None, send(g, 13, line, line, x_recv.at[i, 1], xs[2], y, c)))
            add((None, send(g, 14, passing, line, x_recv.at[i, 2], xs[1], y, c)))
            add((None, send(g, 15, passing, line, x_recv.at[i, 0], xs[3], y, c)))
            add((None, to_partner(g, 12, kv_at(g, c, x, ys[2]))))
        if step == 4:
            for k in range(3):
                add((None, to_partner(g, 16 + k, kv_at(g, c, xs[k + 1], 0, SIDE))))
        return mine

    def arriving(g, step):
        if g in ROW_FIRST:
            i = ROW_FIRST.index(g)
            if step == 2:
                for k in range(3):
                    arrived(kv_at(g, c, xs[k + 1], y), row_recv.at[i, k])

                @pl.when(other_kind)
                def _():
                    arrived(kv_at(g, c, x, y), dd_own.at[g])

            if step == 3:
                arrived(kv_at(g, c, 0, ys[3], SIDE), y_recv.at[i, 0])
                arrived(kv_at(g, c, 0, ys[1], SIDE), y_recv.at[i, 1])
            if step == 4:
                arrived(kv_at(g, c, 0, ys[2], 2), y2_recv.at[i, 0])
                arrived(kv_at(g, c, 2, ys[2], 2), y2_recv.at[i, 1])
            return
        i = COLUMN_FIRST.index(g)
        if step == 2:
            arrived(kv_at(g, c, x, ys[3]), col_recv.at[i, 0])
            arrived(transit_at(g, c, ys[1]), col_recv.at[i, 4])
            arrived(kv_at(g, c, x, ys[1]), col_recv.at[i, 1])
            arrived(transit_at(g, c, ys[3]), col_recv.at[i, 3])
        if step == 3:
            arrived(kv_at(g, c, x, ys[2]), col_recv.at[i, 2])
            arrived(transit_at(g, c, ys[2]), col_recv.at[i, 5])

            @pl.when(own_kind)
            def _():
                arrived(transit_at(g, c, y), dd_own.at[g])

            @pl.when(other_kind)
            def _():
                arrived(kv_at(g, c, x, y), dd_own.at[g])

        if step == 4:
            for k in range(3):
                arrived(kv_at(g, c, xs[k + 1], 0, SIDE), x_recv.at[i, k])

    def go(copies, wait=False):
        for cond, copy in copies:
            act = copy.wait_send if wait else copy.start
            if cond is None:
                act()
            else:
                pl.when(cond)(act)

    def relay(g, step):
        arriving(g, step)
        go(leaving(g, step))

    def complete(g):
        n = 15 * halves[g]
        arrived(keys_values.at[aligned(sp_size * starts[g], n)], dd_all.at[g])

        @pl.when(other_kind)
        def _():
            arrived(kv_at(g, 1 - c, x, y), dd_ownb.at[g])

    def hand_out(g, keys, values):
        n = halves[g]
        stage[starts[g] : starts[g] + sizes[g], :head] = keys
        stage[starts[g] : starts[g] + sizes[g], head:] = values
        go(leaving(g, 1))

        @pl.when(own_kind)
        def _():
            for q in range(2):
                place = kv_at(g, q, x, y)
                place[:, :head] = keys[q * n : (q + 1) * n]
                place[:, head:] = values[q * n : (q + 1) * n]

        if g in COLUMN_FIRST:
            for q in range(2):

                @pl.when(other_kind & (c == q))
                def _():
                    place = transit_at(g, q, y)
                    place[:, :head] = keys[q * n : (q + 1) * n]
                    place[:, head:] = values[q * n : (q + 1) * n]

    def q_copy(g):
        n = sizes[g] if g else pair
        place = aligned(q_starts[g], n)
        return remote(
            q_stage.at[place],
            queries.at[place],
            q_send.at[g],
            q_recv.at[g],
            x + 1 - 2 * p,
            y,
            z,
            1 - c,
        )

    def hand_query(start, found):
        n = found.shape[0]

        @pl.when(own_kind)
        def _():
            queries[aligned(start, n), :] = found

        @pl.when(other_kind)
        def _():
            q_stage[aligned(start, n), :] = found

    quarter = half // 4
    lane = lax.broadcasted_iota(jnp.int32, (pair, half), 1)
    by_row = lane < half // 2
    low = lax.rem(lax.broadcasted_iota(jnp.int32, (1, half), 1), 2 * quarter) < quarter
    factor = half ** (-0.5) * LOG2E

    def angles(blocks):
        found = []
        for row_table, col_table in ((row_cos, col_cos), (row_sin, col_sin)):
            found.append(
                jnp.concatenate(
                    [
                        jnp.where(by_row, row_table[pl.ds(s * chips + b, 1), :], col_table[...])
                        for b in blocks
                    ],
                    axis=0,
                )
            )
        return found

    def turn(raw, cos, sin, scale=None):
        parts = []
        for i in range(head // half):
            v = raw[:, i * half : (i + 1) * half].astype(jnp.bfloat16).astype(jnp.float32)
            other = jnp.where(low, pltpu.roll(v, half - quarter, 1), pltpu.roll(v, quarter, 1))
            turned = v * cos + other * sin
            if scale is not None:
                turned = turned * scale
            parts.append(turned.astype(jnp.bfloat16))
        return jnp.concatenate(parts, axis=1)

    def from_partner(b):
        for part in range(2):
            token_copy(2, b, 1 - c, part).wait_recv()

    forward(2, True)
    from_partner(z)
    locals_[2].wait()
    normalise(context_tokens, 0, 0, ctx_rows, 1)
    normalise(tokens, z * pair, ctx_rows, pair, 0)
    for i in (3, 4, 5):
        locals_[i].wait()
    cos, sin = angles([z])
    found = jnp.dot(normed[: sizes[0], :], wk[...], preferred_element_type=jnp.float32)
    keys = jnp.concatenate([found[:ctx_rows].astype(jnp.bfloat16), turn(found[ctx_rows:], cos, sin)], axis=0)
    values = jnp.dot(normed[: sizes[0], :], wv[...], preferred_element_type=jnp.float32).astype(jnp.bfloat16)
    hand_out(0, keys, values)
    found = jnp.dot(normed[ctx_rows : sizes[0], :], wq[...], preferred_element_type=jnp.float32)
    hand_query(0, turn(found, cos, sin, factor))
    pl.when(other_kind)(lambda: q_copy(0).start())
    forward(2, False)

    def process(d, carry):
        left = ring(z - d, chips)
        right = ring(z + d, chips)

        @pl.when(d == 3)
        def _():
            forward(3, True)
            forward(3, False)

        from_partner(left)
        from_partner(right)
        normalise(tokens, left * pair, 0, pair, 0)
        normalise(tokens, right * pair, pair, pair, 0)
        cos, sin = angles([left, right])
        v = normed[: 2 * pair, :]
        keys = turn(jnp.dot(v, wk[...], preferred_element_type=jnp.float32), cos, sin)
        values = jnp.dot(v, wv[...], preferred_element_type=jnp.float32).astype(jnp.bfloat16)
        for g in (1, 2, 3):
            pl.when(d == g)(functools.partial(hand_out, g, keys, values))
        found = jnp.dot(v, wq[...], preferred_element_type=jnp.float32)
        hand_query(pair + (d - 1) * 2 * pair, turn(found, cos, sin, factor))
        for g in (1, 2, 3):
            pl.when(other_kind & (d == g))(lambda g=g: q_copy(g).start())

        @pl.when(d == 1)
        def _():
            relay(0, 2)

        @pl.when(d == 2)
        def _():
            relay(0, 3)

        @pl.when(d == 3)
        def _():
            relay(1, 2)

        return carry

    lax.fori_loop(1, 4, process, 0)

    opposite = ring(z + far, chips)
    for part in range(2):
        token_copy(2, opposite, c, part).wait_recv()
        token_copy(2, opposite, c, part).start()
    relay(0, 4)
    from_partner(opposite)
    normalise(tokens, opposite * pair, 0, pair, 0)
    cos, sin = angles([opposite])
    v = normed[:pair, :]
    keys = turn(jnp.dot(v, wk[...], preferred_element_type=jnp.float32), cos, sin)
    values = jnp.dot(v, wv[...], preferred_element_type=jnp.float32).astype(jnp.bfloat16)
    hand_out(4, keys, values)
    found = jnp.dot(v, wq[...], preferred_element_type=jnp.float32)
    hand_query(q_starts[4], turn(found, cos, sin, factor))
    pl.when(other_kind)(lambda: q_copy(4).start())

    relay(1, 3)
    relay(2, 2)

    peak[...] = jnp.full(peak.shape, -jnp.inf, jnp.float32)
    total_weight[...] = jnp.zeros(total_weight.shape, jnp.float32)
    mixed[...] = jnp.zeros(mixed.shape, jnp.float32)

    @pl.when(other_kind)
    def _():
        for g in range(5):
            n = sizes[g] if g else pair
            place = queries.at[aligned(q_starts[g], n)]
            remote(place, place, q_send.at[g], q_recv.at[g], x, y, z, 1 - c).wait_recv()

    my_head = 2 * z + p
    weight_of_second = mod_pieces[my_head, 6:7, 0:1]
    lifted = mod_pieces[my_head, 7:8, 0:1] * LOG2E

    def attend(base, count, first_row, n, raised=None):
        keys_at = aligned(base, count)
        at = slice(first_row, first_row + n)
        scores = [
            lax.dot_general(
                queries[at, m * half : (m + 1) * half],
                keys_values[keys_at, m * half : (m + 1) * half],
                (((1,), (1,)), ((), ())),
                preferred_element_type=jnp.float32,
            )
            for m in range(2)
        ]
        for m in range(2):
            score = scores[m] if raised is None else scores[m] + raised
            old = peak[m, at, :]
            new = jnp.maximum(old, jnp.max(score, axis=1, keepdims=True))
            alpha = jnp.exp2(old - new)
            weights = jnp.exp2(score - new[:, :1])
            total_weight[m, at, :] = total_weight[m, at, :] * alpha + jnp.sum(
                weights, axis=1, keepdims=True
            )
            peak[m, at, :] = new
            mixed[m, at, :] = mixed[m, at, :] * alpha[:, :1] + jnp.dot(
                weights.astype(jnp.bfloat16),
                keys_values[keys_at, head:],
                preferred_element_type=jnp.float32,
            )

    def out_copy(i, first_row, n):
        return remote(
            out_stage.at[first_row : first_row + n],
            attended.at[first_row : first_row + n],
            out_send.at[i],
            out_recv.at[i],
            x + 1 - 2 * p,
            y,
            z,
            1 - c,
        )

    tiles = ((q_starts[3], 3 * pair), (0, q_starts[3]))

    def finish(i):
        first_row, n = tiles[i]
        at = slice(first_row, first_row + n)
        diff = mixed[0, at, :] / total_weight[0, at, :1] - weight_of_second * (
            mixed[1, at, :] / total_weight[1, at, :1]
        )
        mean = jnp.sum(diff * diff, axis=1, keepdims=True) * (1.0 / head)
        found = (diff * lax.rsqrt(mean + EPSILON) * gain[...]).astype(jnp.bfloat16)

        @pl.when(own_kind)
        def _():
            attended[at, :] = found

        @pl.when(other_kind)
        def _():
            out_stage[at, :] = found
            out_copy(i, first_row, n).start()

    complete(0)
    count = sp_size * sizes[0]
    column = lax.broadcasted_iota(jnp.int32, (1, count), 1)
    on_context = (column < count // 2) & (lax.rem(column, halves[0]) < ctx_rows)
    attend(0, count, 0, block_tokens, jnp.where(on_context, lifted, 0.0))
    relay(2, 3)
    relay(1, 4)
    relay(3, 2)

    def groups(g, carry):
        for k in (1, 2, 3):
            pl.when(g == k)(functools.partial(complete, k))
        attend(sp_size * (starts[1] + (g - 1) * sizes[1]), sp_size * sizes[1], 0, block_tokens)

        @pl.when(g == 1)
        def _():
            relay(3, 3)
            relay(2, 4)
            relay(4, 2)

        @pl.when(g == 2)
        def _():
            relay(4, 3)
            relay(3, 4)
            relay(4, 4)

        return carry

    lax.fori_loop(1, 4, groups, 0)
    complete(4)
    locals_[6].wait()
    for i in range(2):
        attend(sp_size * starts[4], sp_size * sizes[4], tiles[i][0], tiles[i][1])
        finish(i)

    span = width // 2
    chunk = 1024

    def pair_copy(u):
        ref = pair_send.at[u]
        return remote(ref, pair_recv.at[u], ps_sem.at[u], pr_sem.at[u], x, y, z, 1 - c)

    def ring_copy(side, d, part):
        u = 2 * d + part
        into = (from_left, from_right)[side]
        sem = (left_sem, right_sem)[side]
        to = (ring(z + 1, chips), ring(z - 1, chips))[side]
        v = 2 * (d - 1) + part
        return remote(
            ring_stage.at[side, u], into.at[v], st_sem.at[side, u], sem.at[v], x, y, to, c
        )

    def ring_arrived(side, d, part):
        v = 2 * d + part
        into = (from_left, from_right)[side]
        sem = (left_sem, right_sem)[side]
        remote(into.at[v], into.at[v], st_sem.at[side, v], sem.at[v], x, y, z, 1 - c).wait_recv()

    def block_of(side, d):
        if d == 0:
            return 0
        if d == far:
            return 2 * far - 1
        return 2 * d if side == 0 else 2 * d - 1

    def compute(d):
        blocks = [block_of(0, d)] if d in (0, far) else [block_of(1, d), block_of(0, d)]
        others = [attended[aligned(j * pair + (1 - c) * rows, rows), :] for j in blocks]
        mines = [attended[aligned(j * pair + c * rows, rows), :] for j in blocks]
        both = jnp.concatenate(others + mines, axis=0)
        n = len(blocks)
        for part in range(2):
            for k in range(span // chunk):
                found = jnp.dot(
                    both,
                    wo[:, part * span + k * chunk : part * span + (k + 1) * chunk],
                    preferred_element_type=jnp.float32,
                )
                cols = slice(k * chunk, (k + 1) * chunk)
                for i, j in enumerate(blocks):
                    pair_send[2 * j + part, :, cols] = found[i * rows : (i + 1) * rows].astype(jnp.bfloat16)
                    own[2 * j + part, :, cols] = found[(n + i) * rows : (n + i + 1) * rows]
            for j in blocks:
                pair_copy(2 * j + part).start()

    def combine(side, d, part):
        u = 2 * block_of(side, d) + part
        pair_copy(u).wait_recv()
        value = own[u] + pair_recv[u].astype(jnp.float32)
        if not (d == far or (d == far - 1 and part != side)):
            ring_arrived(side, d, part)
            value = value + (from_left, from_right)[side][2 * d + part].astype(jnp.float32)
        ring_stage[side, 2 * d + part] = value.astype(jnp.bfloat16)
        ring_copy(side, d, part).start()

    @pl.when(other_kind)
    def _():
        first_row, n = tiles[0]
        out_copy(0, first_row, n).wait_recv()

    compute(4)
    compute(3)
    combine(0, 4, 0)
    combine(1, 4, 1)
    combine(0, 3, 1)
    combine(1, 3, 0)

    @pl.when(other_kind)
    def _():
        first_row, n = tiles[1]
        out_copy(1, first_row, n).wait_recv()

    compute(2)
    combine(0, 3, 0)
    combine(1, 3, 1)
    compute(1)
    for d in (2, 1):
        combine(0, d, 1)
        combine(1, d, 0)
        combine(0, d, 0)
        combine(1, d, 1)
        if d == 2:
            compute(0)

    for part in (1, 0):
        cols = slice(part * span, (part + 1) * span)
        pair_copy(part).wait_recv()
        value = own[part] + pair_recv[part].astype(jnp.float32)
        ring_arrived(0, 0, part)
        value = value + from_left[part].astype(jnp.float32)
        ring_arrived(1, 0, part)
        value = value + from_right[part].astype(jnp.float32)
        result[:, cols] = (
            tokens[aligned(t * rows, rows), cols].astype(jnp.float32) + mod_rows[4:5, cols] * value
        ).astype(jnp.bfloat16)

    for u in range(2 * chips):
        pair_copy(u).wait_send()
    for side in range(2):
        ring_copy(side, far, side).wait_send()
        for d in (1, 2, 3):
            for part in range(2):
                ring_copy(side, d, part).wait_send()
    for part in range(2):
        for d in range(far):
            if d < far - 1 or part == 0:
                token_copy(0, ring(z - d, chips), c, part).wait_send()
            if d < far - 1 or part == 1:
                token_copy(1, ring(z + d, chips), c, part).wait_send()
        for b in range(chips):
            token_copy(2, b, c, part).wait_send()
    for k in range(1, tp_size):
        piece_copy(k, t).wait_send()
    for k in range(1, sp_size):
        part_copy(k, s).wait_send()
    for g in range(5):
        for step in (1, 2, 3, 4):
            go(leaving(g, step), True)

    @pl.when(other_kind)
    def _():
        for g in range(5):
            q_copy(g).wait_send()
        for i in range(2):
            out_copy(i, tiles[i][0], tiles[i][1]).wait_send()


def tables(half):
    quarter = half // 4
    inverse = (ROPE_BASE ** (-np.arange(quarter, dtype=np.float32) / quarter)).astype(np.float32)
    inverse = np.tile(inverse, 4)
    sign = np.where(np.arange(half) % (2 * quarter) < quarter, -1.0, 1.0).astype(np.float32)
    found = []
    for count in (8192 // GRID_W, GRID_W):
        angle = np.arange(count, dtype=np.float32)[:, None] * inverse[None, :]
        found.append(np.cos(angle).astype(np.float32))
        found.append((np.sin(angle) * sign).astype(np.float32))
    return found


def shards(
    sp_size,
    tp_size,
    latent,
    context,
    condition,
    context_condition,
    modulation,
    query_weight,
    key_weight,
    value_weight,
    lambdas,
    context_lift,
    head_gain,
    output_weight,
):
    rows, width = latent.shape
    chips = tp_size // 2
    head = query_weight.shape[1]
    half = head // 2
    pair = 2 * rows
    block_tokens = rows * tp_size
    ctx_rows = context.shape[0]
    piece = modulation.shape[2]
    vmem = pl.BlockSpec(memory_space=pltpu.VMEM)
    smem = pl.BlockSpec(memory_space=pltpu.SMEM)
    anywhere = pl.BlockSpec(memory_space=pl.ANY)
    bf16, f32 = jnp.bfloat16, jnp.float32
    dma = pltpu.SemaphoreType.DMA
    blocks = (2 * chips, rows, width // 2)
    row_cos, row_sin, col_cos, col_sin = tables(half)
    return pl.pallas_call(
        functools.partial(kernel, sp_size, tp_size),
        out_shape=jax.ShapeDtypeStruct((rows, width), bf16),
        in_specs=[anywhere] * 2 + [vmem] * 2 + [anywhere] * 4 + [vmem] * 4 + [smem] * 2 + [vmem, anywhere],
        out_specs=vmem,
        scratch_shapes=[
            pltpu.VMEM((block_tokens, width), bf16),
            pltpu.VMEM(context.shape, bf16),
            pltpu.VMEM((2 * pair, width), bf16),
            pltpu.VMEM(modulation.shape, bf16),
            pltpu.VMEM((width, head), bf16),
            pltpu.VMEM((width, head), bf16),
            pltpu.VMEM((width, head), bf16),
            pltpu.VMEM((head, width), bf16),
            pltpu.VMEM((sp_size * (ctx_rows + block_tokens), 2 * head), bf16),
            pltpu.VMEM((SIDE * (ctx_rows + 3 * pair), 2 * head), bf16),
            pltpu.VMEM((ctx_rows + block_tokens, 2 * head), bf16),
            pltpu.VMEM((block_tokens, head), bf16),
            pltpu.VMEM((block_tokens, head), bf16),
            pltpu.VMEM((2, block_tokens, 128), f32),
            pltpu.VMEM((2, block_tokens, 128), f32),
            pltpu.VMEM((2, block_tokens, head), f32),
            pltpu.VMEM((block_tokens, head), bf16),
            pltpu.VMEM((block_tokens, head), bf16),
            pltpu.VMEM((sp_size, 8, piece), f32),
            pltpu.VMEM((tp_size, 8, piece), f32),
            pltpu.VMEM((8, width), f32),
            pltpu.VMEM(blocks, f32),
            pltpu.VMEM(blocks, bf16),
            pltpu.VMEM(blocks, bf16),
            pltpu.VMEM((2, chips + 2, rows, width // 2), bf16),
            pltpu.VMEM((chips, rows, width // 2), bf16),
            pltpu.VMEM((chips, rows, width // 2), bf16),
            dma((7,)),
            dma((3, 2 * chips)),
            dma((2 * tp_size,)),
            dma((sp_size,)),
            dma((sp_size,)),
            dma((tp_size,)),
            dma((tp_size,)),
            dma((5, 19)),
            dma((3, 3)),
            dma((3, 2)),
            dma((3, 2)),
            dma((2, 6)),
            dma((2, 3)),
            dma((5,)),
            dma((5,)),
            dma((5,)),
            dma((5,)),
            dma((5,)),
            dma((2,)),
            dma((2,)),
            dma((2 * chips,)),
            dma((2 * chips,)),
            dma((2, chips + 2)),
            dma((chips,)),
            dma((chips,)),
        ],
        compiler_params=pltpu.CompilerParams(
            collective_id=0, has_side_effects=True, vmem_limit_bytes=VMEM_LIMIT
        ),
        name="layer",
    )(
        latent,
        context,
        condition.reshape(1, -1),
        context_condition.reshape(1, -1),
        modulation,
        query_weight,
        key_weight,
        value_weight,
        jnp.asarray(row_cos),
        jnp.asarray(row_sin),
        jnp.asarray(col_cos),
        jnp.asarray(col_sin),
        lambdas,
        context_lift,
        head_gain.reshape(1, -1),
        output_weight,
    )


def solution(mesh):
    in_specs = (
        P(("sp", "tp"), None),
        P("sp", None),
        P(),
        P(),
        P(None, "sp", "tp"),
        P(None, "tp"),
        P(None, "tp"),
        P(None, "tp"),
        P("tp"),
        P("tp"),
        P(),
        P("tp", None),
    )
    out_specs = P(("sp", "tp"), None)
    body = functools.partial(shards, mesh.shape["sp"], mesh.shape["tp"])
    return jax.shard_map(body, mesh=mesh, in_specs=in_specs, out_specs=out_specs, check_vma=False)
```

time: 202 us -> 119 us (0.59)
  Pallas kernels: 197 us -> 116 us
  other arithmetic: 2.09 us -> 0 us
    pallas_call x2 -> x1, Pallas kernels: 197 us -> 116 us  [shards(): pl.pallas_call(functools.partial(kernel, sp_size, tp_size), out_shape=jax...]
    mul x2 -> x0, other arithmetic: 2.06 us -> none  [the longest x1 1.86 us: tables(): return (jnp.cos(angles), jnp.sin(angles) * sign)]
where the time goes in v1:
time: 119 us
  Pallas kernels  116 us (97%)
  local copies, waits for them, and re-layouts  1.67 us (1%)
  between operations  1.31 us (1%)
    pallas_call x1, Pallas kernels, shards(): pl.pallas_call(functools.partial(kernel, sp_size, tp_size), out_shape=jax...  116 us

profile of v1, /device:TPU:1, one launch (start us, length us, event | category | flops | bytes accessed | tf_op | source)
XLA Modules:
  0.0 119.3 jit_solution(13721886423243808236)
XLA Ops:
  1.3 116.3 %layer.1 = bf16[32,4096]{1,0:T(8,128)(2,1)} custom-call(bf16[32,4096]{1,0:T(8,128)(2,1)} %latent.1, bf16[32,4096]{1,0:T(8,128)(2,1)} %context.1, f32[1,4096]{1,0:T(1,128)} %bitcast.3, f32[1,4096]{1,0:T(1,128)} %bitcast.4, bf16[3,256,256]{2,1,0:T(8,128)(2,1)} %modulation.1, bf16[4096,256]{1,0:T(8,128)(2,1)} %query_weight.1, bf16[4096,256]{1,0:T(8,128)(2,1)} %key_weight.1, ...), custom_call_target="tpu_custom_call" | custom-call | tf_op jit(solution)/shard_map/layer/pallas_call | solution.py:868
  117.6 1.7 %copy.20 = bf16[32,4096]{1,0:T(8,128)(2,1)} copy(bf16[32,4096]{1,0:T(8,128)(2,1)} %layer.1) | data formatting | bytes 524288

commit v2 on v1

--- a/solution.py
+++ b/solution.py
@@ -16,8 +16,7 @@
 SIDE = 4
 VMEM_LIMIT = 63 * 1024 * 1024
 MESH = pl.DeviceIdType.MESH
-ROW_FIRST = (1, 3, 4)
-COLUMN_FIRST = (0, 2)
+GROUPS = 5
 
 
 def aligned(start, size, unit=ROWS):
@@ -225,9 +224,9 @@
 
     for k in range(1, sp_size):
         part_copy(k, s).start()
+    token_copy(0, z, c, 0).start()
+    token_copy(1, z, c, 1).start()
     for part in range(2):
-        token_copy(0, z, c, part).start()
-        token_copy(1, z, c, 1 - part).start()
         token_copy(2, z, c, part).start()
 
     for k in range(1, sp_size):
@@ -238,8 +237,10 @@
     mod_pieces[t] = total
     mod_pieces[t, 6:7, :] = jnp.full((1, piece), lambdas[0], jnp.float32)
     mod_pieces[t, 7:8, :] = jnp.full((1, piece), lift[0], jnp.float32)
-    for k in range(1, tp_size):
+    for k in sorted(range(1, tp_size), key=lambda k: -min(k, tp_size - k)):
         piece_copy(k, t).start()
+    token_copy(0, z, c, 1).start()
+    token_copy(1, z, c, 0).start()
 
     def forward(d, early):
         left = ring(z - d, chips)
@@ -255,45 +256,41 @@
         token_copy(2, right, c, left_part).start()
 
     forward(1, True)
-    forward(1, False)
     for k in range(1, tp_size):
         piece_copy(k, lax.rem(t + k, tp_size)).wait_recv()
     for i in range(tp_size):
         mod_rows[:, i * piece : (i + 1) * piece] = mod_pieces[i]
 
     def normalise(source, base, dest, count, row):
-        def group(i, carry):
-            v = source[aligned(base + i * ROWS, ROWS), :].astype(jnp.float32)
-            v = v - jnp.sum(v, axis=1, keepdims=True) * (1.0 / width)
-            spread = jnp.sum(v * v, axis=1, keepdims=True) * (1.0 / width)
-            v = v * lax.rsqrt(spread + EPSILON)
-            v = v * (1.0 + mod_rows[2 + row : 3 + row, :]) + mod_rows[row : row + 1, :]
-            normed[aligned(dest + i * ROWS, ROWS), :] = v.astype(jnp.bfloat16)
-            return carry
-
-        lax.fori_loop(0, count // ROWS, group, 0)
+        v = source[aligned(base, count), :].astype(jnp.float32)
+        v = v - jnp.sum(v, axis=1, keepdims=True) * (1.0 / width)
+        spread = jnp.sum(v * v, axis=1, keepdims=True) * (1.0 / width)
+        v = v * lax.rsqrt(spread + EPSILON)
+        v = v * (1.0 + mod_rows[2 + row : 3 + row, :]) + mod_rows[row : row + 1, :]
+        normed[aligned(dest, count), :] = v.astype(jnp.bfloat16)
 
     sizes = (ctx_rows + pair, 2 * pair, 2 * pair, 2 * pair, pair)
-    starts = tuple(sum(sizes[:g]) for g in range(5))
-    q_starts = (0, pair, 3 * pair, 5 * pair, 7 * pair)
-    transit_starts = {0: 0, 2: SIDE * sizes[0]}
-    halves = tuple(n // 2 for n in sizes)
+    starts = tuple(sum(sizes[:g]) for g in range(GROUPS))
+    firsts = (pair, pair, pair, pair, pair // 2)
+    halves = tuple((firsts[g], sizes[g] - firsts[g]) for g in range(GROUPS))
+    transit_starts = tuple(SIDE * sum(h[1] for h in halves[:g]) for g in range(GROUPS))
     own_kind = p == c
     other_kind = p != c
     xs = [x, lax.rem(x + 1, SIDE), lax.rem(x + 2, SIDE), lax.rem(x + 3, SIDE)]
     ys = [y, lax.rem(y + 1, SIDE), lax.rem(y + 2, SIDE), lax.rem(y + 3, SIDE)]
 
     def kv_at(g, q, sx, sy, count=1):
-        order = sy * SIDE + sx if g in ROW_FIRST else sx * SIDE + sy
-        n = halves[g]
-        return keys_values.at[aligned(sp_size * starts[g] + (q * sp_size + order) * n, count * n)]
-
-    def transit_at(g, q, sy, count=1):
-        n = halves[g]
-        return transit.at[aligned(transit_starts[g] + (q * SIDE + sy) * n, count * n)]
+        n = halves[g][q]
+        order = sx * SIDE + sy if q else sy * SIDE + sx
+        start = sp_size * (starts[g] + q * halves[g][0])
+        return keys_values.at[aligned(start + order * n, count * n)]
+
+    def transit_at(g, sy, count=1):
+        n = halves[g][1]
+        return transit.at[aligned(transit_starts[g] + sy * n, count * n)]
 
     def stage_at(g, q):
-        return stage.at[aligned(starts[g] + q * halves[g], halves[g])]
+        return stage.at[aligned(starts[g] + q * halves[g][0], halves[g][q])]
 
     def send(g, k, src, dst, recv_sem, sx, sy, sc):
         return remote(src, dst, kv_send.at[g, k], recv_sem, sx, sy, z, sc)
@@ -304,102 +301,105 @@
     def arrived(ref, recv_sem):
         remote(ref, ref, kv_send.at[0, 0], recv_sem, x, y, z, 1 - c).wait_recv()
 
-    def leaving(g, step):
+    def leaving(g, step, core=None):
         mine = []
-        add = mine.append
-        if g in ROW_FIRST:
-            i = ROW_FIRST.index(g)
-            if step == 1:
-                for q in range(2):
-                    there = kv_at(g, q, x, y)
-                    add((other_kind, send(g, q, stage_at(g, q), there, row_recv.at[i, 2], xs[1], y, q)))
-                    add((other_kind, send(g, 2 + q, stage_at(g, q), there, row_recv.at[i, 0], xs[3], y, q)))
-                    add((own_kind, send(g, 4 + q, stage_at(g, q), there, row_recv.at[i, 1], xs[2], y, q)))
-                add((own_kind, send(g, 6, stage_at(g, 1 - c), kv_at(g, 1 - c, x, y), dd_own.at[g], x, y, 1 - c)))
-                add((own_kind, send(g, 7, stage_at(g, c), kv_at(g, c, x, y), dd_ownb.at[g], x, y, 1 - c)))
+
+        def add(cond, *args):
+            mine.append((cond, send(g, *args)))
+
+        def on(k, ref):
+            mine.append((None, to_partner(g, k, ref)))
+
+        if step == 1:
+            for q, owner in ((0, 0), (1, 1)):
+                here = stage_at(g, q)
+                if q == 0:
+                    there = kv_at(g, 0, x, y)
+                    add(other_kind, 0, here, there, row_recv.at[g, 2], xs[1], y, owner)
+                    add(other_kind, 1, here, there, row_recv.at[g, 0], xs[3], y, owner)
+                    add(own_kind, 0, here, there, row_recv.at[g, 1], xs[2], y, owner)
+                    continue
+                for kind, cond, there in ((0, own_kind, kv_at(g, 1, x, y)), (1, other_kind, transit_at(g, y))):
+                    add(cond, 2, here, there, col_recv.at[g, 3 * kind], x, ys[1], owner)
+                    add(cond, 3, here, there, col_recv.at[g, 3 * kind + 1], x, ys[3], owner)
+            for q in range(2):
+                cond = own_kind & (c == q)
+                add(cond, 4, stage_at(g, 1 - q), kv_at(g, 1 - q, x, y), dd_own.at[g], x, y, 1 - c)
+                add(cond, 5, stage_at(g, q), kv_at(g, q, x, y), dd_ownb.at[g], x, y, 1 - c)
+            add(other_kind & (c == 0), 4, stage_at(g, 1), transit_at(g, y), dd_own.at[g], x, y, 1 - c)
+        elif core == 0:
             if step == 2:
-                line = kv_at(g, c, 0, y, SIDE)
-                add((None, send(g, 11, line, line, y_recv.at[i, 0], x, ys[1], c)))
-                add((None, send(g, 12, line, line, y_recv.at[i, 1], x, ys[3], c)))
+                line = kv_at(g, 0, 0, y, SIDE)
+                add(None, 6, line, line, y_recv.at[g, 0], x, ys[1], 0)
+                add(None, 7, line, line, y_recv.at[g, 1], x, ys[3], 0)
                 for k in range(3):
-                    add((None, to_partner(g, 8 + k, kv_at(g, c, xs[k + 1], y))))
+                    on(8 + k, kv_at(g, 0, xs[k + 1], y))
             if step == 3:
-                low = kv_at(g, c, 0, ys[3], 2)
-                high = kv_at(g, c, 2, ys[1], 2)
-                add((None, send(g, 15, low, low, y2_recv.at[i, 0], x, ys[1], c)))
-                add((None, send(g, 16, high, high, y2_recv.at[i, 1], x, ys[3], c)))
-                add((None, to_partner(g, 13, kv_at(g, c, 0, ys[3], SIDE))))
-                add((None, to_partner(g, 14, kv_at(g, c, 0, ys[1], SIDE))))
+                low = kv_at(g, 0, 0, ys[3], 2)
+                high = kv_at(g, 0, 2, ys[1], 2)
+                add(None, 11, low, low, y2_recv.at[g, 0], x, ys[1], 0)
+                add(None, 12, high, high, y2_recv.at[g, 1], x, ys[3], 0)
+                on(13, kv_at(g, 0, 0, ys[3], SIDE))
+                on(14, kv_at(g, 0, 0, ys[1], SIDE))
             if step == 4:
-                add((None, to_partner(g, 17, kv_at(g, c, 0, ys[2], SIDE))))
-            return mine
-        i = COLUMN_FIRST.index(g)
-        if step == 1:
-            for q in range(2):
-                for kind, cond, there in ((0, own_kind, kv_at(g, q, x, y)), (1, other_kind, transit_at(g, q, y))):
-                    add((cond, send(g, q, stage_at(g, q), there, col_recv.at[i, 3 * kind], x, ys[1], q)))
-                    add((cond, send(g, 2 + q, stage_at(g, q), there, col_recv.at[i, 3 * kind + 1], x, ys[3], q)))
-            add((own_kind, send(g, 6, stage_at(g, 1 - c), kv_at(g, 1 - c, x, y), dd_own.at[g], x, y, 1 - c)))
-            add((other_kind, send(g, 6, stage_at(g, 1 - c), transit_at(g, 1 - c, y), dd_own.at[g], x, y, 1 - c)))
-            add((own_kind, send(g, 7, stage_at(g, c), kv_at(g, c, x, y), dd_ownb.at[g], x, y, 1 - c)))
+                on(15, kv_at(g, 0, 0, ys[2], SIDE))
+        else:
+            if step == 2:
+                below = kv_at(g, 1, x, ys[3])
+                above = transit_at(g, ys[1])
+                add(None, 6, below, below, col_recv.at[g, 2], x, ys[1], 1)
+                add(None, 7, above, above, col_recv.at[g, 5], x, ys[3], 1)
+                on(8, below)
+                on(9, kv_at(g, 1, x, ys[1]))
+            if step == 3:
+                line = kv_at(g, 1, x, 0, SIDE)
+                passing = transit_at(g, 0, SIDE)
+                add(None, 10, line, line, x_recv.at[g, 1], xs[2], y, 1)
+                add(None, 11, passing, line, x_recv.at[g, 2], xs[1], y, 1)
+                add(None, 12, passing, line, x_recv.at[g, 0], xs[3], y, 1)
+                on(13, kv_at(g, 1, x, ys[2]))
+            if step == 4:
+                for k in range(3):
+                    on(14 + k, kv_at(g, 1, xs[k + 1], 0, SIDE))
+        return mine
+
+    def arriving(g, step, core):
+        if core == 0:
+            if step == 2:
+                for k in range(3):
+                    arrived(kv_at(g, 0, xs[k + 1], y), row_recv.at[g, k])
+
+                @pl.when(other_kind)
+                def _():
+                    arrived(kv_at(g, 0, x, y), dd_own.at[g])
+
+            if step == 3:
+                arrived(kv_at(g, 0, 0, ys[3], SIDE), y_recv.at[g, 0])
+                arrived(kv_at(g, 0, 0, ys[1], SIDE), y_recv.at[g, 1])
+            if step == 4:
+                arrived(kv_at(g, 0, 0, ys[2], 2), y2_recv.at[g, 0])
+                arrived(kv_at(g, 0, 2, ys[2], 2), y2_recv.at[g, 1])
+            return
         if step == 2:
-            below = kv_at(g, c, x, ys[3])
-            above = transit_at(g, c, ys[1])
-            add((None, send(g, 9, below, below, col_recv.at[i, 2], x, ys[1], c)))
-            add((None, send(g, 11, above, above, col_recv.at[i, 5], x, ys[3], c)))
-            add((None, to_partner(g, 8, below)))
-            add((None, to_partner(g, 10, kv_at(g, c, x, ys[1]))))
+            arrived(kv_at(g, 1, x, ys[3]), col_recv.at[g, 0])
+            arrived(transit_at(g, ys[1]), col_recv.at[g, 4])
+            arrived(kv_at(g, 1, x, ys[1]), col_recv.at[g, 1])
+            arrived(transit_at(g, ys[3]), col_recv.at[g, 3])
         if step == 3:
-            line = kv_at(g, c, x, 0, SIDE)
-            passing = transit_at(g, c, 0, SIDE)
-            add((None, send(g, 13, line, line, x_recv.at[i, 1], xs[2], y, c)))
-            add((None, send(g, 14, passing, line, x_recv.at[i, 2], xs[1], y, c)))
-            add((None, send(g, 15, passing, line, x_recv.at[i, 0], xs[3], y, c)))
-            add((None, to_partner(g, 12, kv_at(g, c, x, ys[2]))))
+            arrived(kv_at(g, 1, x, ys[2]), col_recv.at[g, 2])
+            arrived(transit_at(g, ys[2]), col_recv.at[g, 5])
+
+            @pl.when(own_kind)
+            def _():
+                arrived(transit_at(g, y), dd_own.at[g])
+
+            @pl.when(other_kind)
+            def _():
+                arrived(kv_at(g, 1, x, y), dd_own.at[g])
+
         if step == 4:
             for k in range(3):
-                add((None, to_partner(g, 16 + k, kv_at(g, c, xs[k + 1], 0, SIDE))))
-        return mine
-
-    def arriving(g, step):
-        if g in ROW_FIRST:
-            i = ROW_FIRST.index(g)
-            if step == 2:
-                for k in range(3):
-                    arrived(kv_at(g, c, xs[k + 1], y), row_recv.at[i, k])
-
-                @pl.when(other_kind)
-                def _():
-                    arrived(kv_at(g, c, x, y), dd_own.at[g])
-
-            if step == 3:
-                arrived(kv_at(g, c, 0, ys[3], SIDE), y_recv.at[i, 0])
-                arrived(kv_at(g, c, 0, ys[1], SIDE), y_recv.at[i, 1])
-            if step == 4:
-                arrived(kv_at(g, c, 0, ys[2], 2), y2_recv.at[i, 0])
-                arrived(kv_at(g, c, 2, ys[2], 2), y2_recv.at[i, 1])
-            return
-        i = COLUMN_FIRST.index(g)
-        if step == 2:
-            arrived(kv_at(g, c, x, ys[3]), col_recv.at[i, 0])
-            arrived(transit_at(g, c, ys[1]), col_recv.at[i, 4])
-            arrived(kv_at(g, c, x, ys[1]), col_recv.at[i, 1])
-            arrived(transit_at(g, c, ys[3]), col_recv.at[i, 3])
-        if step == 3:
-            arrived(kv_at(g, c, x, ys[2]), col_recv.at[i, 2])
-            arrived(transit_at(g, c, ys[2]), col_recv.at[i, 5])
-
-            @pl.when(own_kind)
-            def _():
-                arrived(transit_at(g, c, y), dd_own.at[g])
-
-            @pl.when(other_kind)
-            def _():
-                arrived(kv_at(g, c, x, y), dd_own.at[g])
-
-        if step == 4:
-            for k in range(3):
-                arrived(kv_at(g, c, xs[k + 1], 0, SIDE), x_recv.at[i, k])
+                arrived(kv_at(g, 1, xs[k + 1], 0, SIDE), x_recv.at[g, k])
 
     def go(copies, wait=False):
         for cond, copy in copies:
@@ -409,64 +409,60 @@
             else:
                 pl.when(cond)(act)
 
-    def relay(g, step):
-        arriving(g, step)
-        go(leaving(g, step))
+    def relay(core, *stages):
+        @pl.when(c == core)
+        def _():
+            for g, step in stages:
+                arriving(g, step, core)
+                go(leaving(g, step, core))
 
     def complete(g):
-        n = 15 * halves[g]
-        arrived(keys_values.at[aligned(sp_size * starts[g], n)], dd_all.at[g])
-
-        @pl.when(other_kind)
-        def _():
-            arrived(kv_at(g, 1 - c, x, y), dd_ownb.at[g])
+        for core in range(2):
+
+            @pl.when(c == core)
+            def _():
+                q = 1 - core
+                n = 15 * halves[g][q]
+                start = sp_size * (starts[g] + q * halves[g][0])
+                arrived(keys_values.at[start : start + n], dd_all.at[g])
+
+                @pl.when(other_kind)
+                def _():
+                    arrived(kv_at(g, q, x, y), dd_ownb.at[g])
 
     def hand_out(g, keys, values):
-        n = halves[g]
         stage[starts[g] : starts[g] + sizes[g], :head] = keys
         stage[starts[g] : starts[g] + sizes[g], head:] = values
         go(leaving(g, 1))
+        parts = (slice(0, halves[g][0]), slice(halves[g][0], sizes[g]))
 
         @pl.when(own_kind)
         def _():
             for q in range(2):
                 place = kv_at(g, q, x, y)
-                place[:, :head] = keys[q * n : (q + 1) * n]
-                place[:, head:] = values[q * n : (q + 1) * n]
-
-        if g in COLUMN_FIRST:
-            for q in range(2):
-
-                @pl.when(other_kind & (c == q))
-                def _():
-                    place = transit_at(g, q, y)
-                    place[:, :head] = keys[q * n : (q + 1) * n]
-                    place[:, head:] = values[q * n : (q + 1) * n]
-
-    def q_copy(g):
-        n = sizes[g] if g else pair
-        place = aligned(q_starts[g], n)
+                place[:, :head] = keys[parts[q]]
+                place[:, head:] = values[parts[q]]
+
+        @pl.when(other_kind & (c == 1))
+        def _():
+            place = transit_at(g, y)
+            place[:, :head] = keys[parts[1]]
+            place[:, head:] = values[parts[1]]
+
+    q_parts = ((0, 5 * pair), (5 * pair, 3 * pair))
+
+    def q_copy(i):
+        place = aligned(*q_parts[i])
         return remote(
             q_stage.at[place],
             queries.at[place],
-            q_send.at[g],
-            q_recv.at[g],
+            q_send.at[i],
+            q_recv.at[i],
             x + 1 - 2 * p,
             y,
             z,
             1 - c,
         )
-
-    def hand_query(start, found):
-        n = found.shape[0]
-
-        @pl.when(own_kind)
-        def _():
-            queries[aligned(start, n), :] = found
-
-        @pl.when(other_kind)
-        def _():
-            q_stage[aligned(start, n), :] = found
 
     quarter = half // 4
     lane = lax.broadcasted_iota(jnp.int32, (pair, half), 1)
@@ -503,7 +499,26 @@
         for part in range(2):
             token_copy(2, b, 1 - c, part).wait_recv()
 
-    forward(2, True)
+    def ask(i, blocks):
+        first_row, n = q_parts[i]
+        at = slice(first_row, first_row + n)
+        cos, sin = angles(blocks)
+        found = jnp.dot(
+            normed[ctx_rows + first_row : ctx_rows + first_row + n, :],
+            wq[...],
+            preferred_element_type=jnp.float32,
+        )
+        found = turn(found, cos, sin, factor)
+
+        @pl.when(own_kind)
+        def _():
+            queries[at, :] = found
+
+        @pl.when(other_kind)
+        def _():
+            q_stage[at, :] = found
+            q_copy(i).start()
+
     from_partner(z)
     locals_[2].wait()
     normalise(context_tokens, 0, 0, ctx_rows, 1)
@@ -515,69 +530,76 @@
     keys = jnp.concatenate([found[:ctx_rows].astype(jnp.bfloat16), turn(found[ctx_rows:], cos, sin)], axis=0)
     values = jnp.dot(normed[: sizes[0], :], wv[...], preferred_element_type=jnp.float32).astype(jnp.bfloat16)
     hand_out(0, keys, values)
-    found = jnp.dot(normed[ctx_rows : sizes[0], :], wq[...], preferred_element_type=jnp.float32)
-    hand_query(0, turn(found, cos, sin, factor))
-    pl.when(other_kind)(lambda: q_copy(0).start())
-    forward(2, False)
+    forward(1, False)
 
     def process(d, carry):
         left = ring(z - d, chips)
         right = ring(z + d, chips)
 
-        @pl.when(d == 3)
-        def _():
-            forward(3, True)
-            forward(3, False)
-
         from_partner(left)
         from_partner(right)
-        normalise(tokens, left * pair, 0, pair, 0)
-        normalise(tokens, right * pair, pair, pair, 0)
+        base = starts[1] + (d - 1) * 2 * pair
+        normalise(tokens, left * pair, base, pair, 0)
+        normalise(tokens, right * pair, base + pair, pair, 0)
+
+        @pl.when(d == 1)
+        def _():
+            forward(2, True)
+
+        @pl.when(d == 2)
+        def _():
+            forward(3, True)
+            relay(0, (0, 2))
+            relay(1, (0, 2))
+
+        @pl.when(d == 3)
+        def _():
+            opposite = ring(z + far, chips)
+            token_copy(2, opposite, c, 0).wait_recv()
+            token_copy(2, opposite, c, 0).start()
+            relay(0, (1, 2))
+            relay(1, (1, 2), (0, 3))
+
         cos, sin = angles([left, right])
-        v = normed[: 2 * pair, :]
+        v = normed[aligned(base, 2 * pair), :]
         keys = turn(jnp.dot(v, wk[...], preferred_element_type=jnp.float32), cos, sin)
         values = jnp.dot(v, wv[...], preferred_element_type=jnp.float32).astype(jnp.bfloat16)
         for g in (1, 2, 3):
             pl.when(d == g)(functools.partial(hand_out, g, keys, values))
-        found = jnp.dot(v, wq[...], preferred_element_type=jnp.float32)
-        hand_query(pair + (d - 1) * 2 * pair, turn(found, cos, sin, factor))
-        for g in (1, 2, 3):
-            pl.when(other_kind & (d == g))(lambda g=g: q_copy(g).start())
 
         @pl.when(d == 1)
         def _():
-            relay(0, 2)
+            forward(2, False)
 
         @pl.when(d == 2)
         def _():
-            relay(0, 3)
-
-        @pl.when(d == 3)
-        def _():
-            relay(1, 2)
+            around = [z]
+            for k in (1, 2):
+                around += [ring(z - k, chips), ring(z + k, chips)]
+            ask(0, around)
+            forward(3, False)
 
         return carry
 
     lax.fori_loop(1, 4, process, 0)
 
     opposite = ring(z + far, chips)
-    for part in range(2):
-        token_copy(2, opposite, c, part).wait_recv()
-        token_copy(2, opposite, c, part).start()
-    relay(0, 4)
+    token_copy(2, opposite, c, 1).wait_recv()
+    token_copy(2, opposite, c, 1).start()
+    relay(0, (2, 2))
     from_partner(opposite)
-    normalise(tokens, opposite * pair, 0, pair, 0)
+    normalise(tokens, opposite * pair, starts[4], pair, 0)
+    relay(1, (2, 2))
     cos, sin = angles([opposite])
-    v = normed[:pair, :]
+    v = normed[starts[4] : starts[4] + pair, :]
     keys = turn(jnp.dot(v, wk[...], preferred_element_type=jnp.float32), cos, sin)
     values = jnp.dot(v, wv[...], preferred_element_type=jnp.float32).astype(jnp.bfloat16)
     hand_out(4, keys, values)
-    found = jnp.dot(v, wq[...], preferred_element_type=jnp.float32)
-    hand_query(q_starts[4], turn(found, cos, sin, factor))
-    pl.when(other_kind)(lambda: q_copy(4).start())
-
-    relay(1, 3)
-    relay(2, 2)
+    relay(0, (0, 3))
+    relay(1, (1, 3))
+    ask(1, [ring(z - 3, chips), ring(z + 3, chips), opposite])
+    relay(0, (3, 2), (4, 2), (1, 3), (2, 3), (0, 4))
+    relay(1, (3, 2), (0, 4), (2, 3), (4, 2), (3, 3), (4, 3))
 
     peak[...] = jnp.full(peak.shape, -jnp.inf, jnp.float32)
     total_weight[...] = jnp.zeros(total_weight.shape, jnp.float32)
@@ -585,10 +607,9 @@
 
     @pl.when(other_kind)
     def _():
-        for g in range(5):
-            n = sizes[g] if g else pair
-            place = queries.at[aligned(q_starts[g], n)]
-            remote(place, place, q_send.at[g], q_recv.at[g], x, y, z, 1 - c).wait_recv()
+        for i in range(2):
+            place = queries.at[aligned(*q_parts[i])]
+            remote(place, place, q_send.at[i], q_recv.at[i], x, y, z, 1 - c).wait_recv()
 
     my_head = 2 * z + p
     weight_of_second = mod_pieces[my_head, 6:7, 0:1]
@@ -596,7 +617,7 @@
 
     def attend(base, count, first_row, n, raised=None):
         keys_at = aligned(base, count)
-        at = slice(first_row, first_row + n)
+        at = aligned(first_row, n)
         scores = [
             lax.dot_general(
                 queries[at, m * half : (m + 1) * half],
@@ -634,7 +655,7 @@
             1 - c,
         )
 
-    tiles = ((q_starts[3], 3 * pair), (0, q_starts[3]))
+    tiles = (q_parts[1], q_parts[0])
 
     def finish(i):
         first_row, n = tiles[i]
@@ -654,40 +675,64 @@
             out_stage[at, :] = found
             out_copy(i, first_row, n).start()
 
-    complete(0)
     count = sp_size * sizes[0]
     column = lax.broadcasted_iota(jnp.int32, (1, count), 1)
-    on_context = (column < count // 2) & (lax.rem(column, halves[0]) < ctx_rows)
-    attend(0, count, 0, block_tokens, jnp.where(on_context, lifted, 0.0))
-    relay(2, 3)
-    relay(1, 4)
-    relay(3, 2)
-
-    def groups(g, carry):
-        for k in (1, 2, 3):
-            pl.when(g == k)(functools.partial(complete, k))
-        attend(sp_size * (starts[1] + (g - 1) * sizes[1]), sp_size * sizes[1], 0, block_tokens)
-
-        @pl.when(g == 1)
-        def _():
-            relay(3, 3)
-            relay(2, 4)
-            relay(4, 2)
-
-        @pl.when(g == 2)
-        def _():
-            relay(4, 3)
-            relay(3, 4)
-            relay(4, 4)
+    on_context = (column < sp_size * halves[0][0]) & (lax.rem(column, halves[0][0]) < ctx_rows)
+    raised = jnp.where(on_context, lifted, 0.0)
+    tile = block_tokens // 2
+
+    complete(0)
+
+    def first_group(i, carry):
+        attend(0, count, i * tile, tile, raised)
+
+        @pl.when(i == 0)
+        def _():
+            relay(0, (3, 3))
 
         return carry
 
-    lax.fori_loop(1, 4, groups, 0)
+    lax.fori_loop(0, 2, first_group, 0)
+    relay(0, (4, 3), (1, 4))
+    relay(1, (1, 4))
+    complete(1)
+
+    def groups(j, carry):
+        g = lax.div(j, 2) + 1
+        i = lax.rem(j, 2)
+        attend(sp_size * (starts[1] + (g - 1) * sizes[1]), sp_size * sizes[1], i * tile, tile)
+
+        @pl.when(j == 0)
+        def _():
+            relay(0, (2, 4))
+            relay(1, (2, 4))
+
+        @pl.when(j == 1)
+        def _():
+            complete(2)
+
+        @pl.when(j == 2)
+        def _():
+            relay(0, (3, 4), (4, 4))
+            relay(1, (3, 4))
+
+        @pl.when(j == 3)
+        def _():
+            relay(1, (4, 4))
+            complete(3)
+
+        return carry
+
+    lax.fori_loop(0, 6, groups, 0)
     complete(4)
     locals_[6].wait()
-    for i in range(2):
+
+    def last_group(i):
         attend(sp_size * starts[4], sp_size * sizes[4], tiles[i][0], tiles[i][1])
         finish(i)
+
+    last_group(0)
+    last_group(1)
 
     span = width // 2
     chunk = 1024
@@ -755,11 +800,13 @@
         out_copy(0, first_row, n).wait_recv()
 
     compute(4)
-    compute(3)
     combine(0, 4, 0)
     combine(1, 4, 1)
+    compute(3)
     combine(0, 3, 1)
     combine(1, 3, 0)
+    combine(0, 3, 0)
+    combine(1, 3, 1)
 
     @pl.when(other_kind)
     def _():
@@ -767,36 +814,10 @@
         out_copy(1, first_row, n).wait_recv()
 
     compute(2)
-    combine(0, 3, 0)
-    combine(1, 3, 1)
+    combine(0, 2, 1)
+    combine(1, 2, 0)
     compute(1)
-    for d in (2, 1):
-        combine(0, d, 1)
-        combine(1, d, 0)
-        combine(0, d, 0)
-        combine(1, d, 1)
-        if d == 2:
-            compute(0)
-
-    for part in (1, 0):
-        cols = slice(part * span, (part + 1) * span)
-        pair_copy(part).wait_recv()
-        value = own[part] + pair_recv[part].astype(jnp.float32)
-        ring_arrived(0, 0, part)
-        value = value + from_left[part].astype(jnp.float32)
-        ring_arrived(1, 0, part)
-        value = value + from_right[part].astype(jnp.float32)
-        result[:, cols] = (
-            tokens[aligned(t * rows, rows), cols].astype(jnp.float32) + mod_rows[4:5, cols] * value
-        ).astype(jnp.bfloat16)
-
-    for u in range(2 * chips):
-        pair_copy(u).wait_send()
-    for side in range(2):
-        ring_copy(side, far, side).wait_send()
-        for d in (1, 2, 3):
-            for part in range(2):
-                ring_copy(side, d, part).wait_send()
+
     for part in range(2):
         for d in range(far):
             if d < far - 1 or part == 0:
@@ -809,16 +830,49 @@
         piece_copy(k, t).wait_send()
     for k in range(1, sp_size):
         part_copy(k, s).wait_send()
-    for g in range(5):
-        for step in (1, 2, 3, 4):
-            go(leaving(g, step), True)
+    combine(0, 2, 0)
+    combine(1, 2, 1)
+    compute(0)
+    for g in range(GROUPS):
+        go(leaving(g, 1), True)
+    for core in range(2):
+
+        @pl.when(c == core)
+        def _():
+            for g in range(GROUPS):
+                for step in (2, 3, 4):
+                    go(leaving(g, step, core), True)
 
     @pl.when(other_kind)
     def _():
-        for g in range(5):
-            q_copy(g).wait_send()
         for i in range(2):
+            q_copy(i).wait_send()
             out_copy(i, tiles[i][0], tiles[i][1]).wait_send()
+
+    for u in range(2 * chips):
+        pair_copy(u).wait_send()
+    combine(0, 1, 1)
+    combine(1, 1, 0)
+    combine(0, 1, 0)
+    combine(1, 1, 1)
+
+    for part in (1, 0):
+        cols = slice(part * span, (part + 1) * span)
+        pair_copy(part).wait_recv()
+        value = own[part] + pair_recv[part].astype(jnp.float32)
+        ring_arrived(0, 0, part)
+        value = value + from_left[part].astype(jnp.float32)
+        ring_arrived(1, 0, part)
+        value = value + from_right[part].astype(jnp.float32)
+        result[:, cols] = (
+            tokens[aligned(t * rows, rows), cols].astype(jnp.float32) + mod_rows[4:5, cols] * value
+        ).astype(jnp.bfloat16)
+
+    for side in range(2):
+        ring_copy(side, far, side).wait_send()
+        for d in (1, 2, 3):
+            for part in range(2):
+                ring_copy(side, d, part).wait_send()
 
 
 def tables(half):
@@ -873,14 +927,14 @@
         scratch_shapes=[
             pltpu.VMEM((block_tokens, width), bf16),
             pltpu.VMEM(context.shape, bf16),
-            pltpu.VMEM((2 * pair, width), bf16),
+            pltpu.VMEM((ctx_rows + block_tokens, width), bf16),
             pltpu.VMEM(modulation.shape, bf16),
             pltpu.VMEM((width, head), bf16),
             pltpu.VMEM((width, head), bf16),
             pltpu.VMEM((width, head), bf16),
             pltpu.VMEM((head, width), bf16),
             pltpu.VMEM((sp_size * (ctx_rows + block_tokens), 2 * head), bf16),
-            pltpu.VMEM((SIDE * (ctx_rows + 3 * pair), 2 * head), bf16),
+            pltpu.VMEM((SIDE * block_tokens // 2, 2 * head), bf16),
             pltpu.VMEM((ctx_rows + block_tokens, 2 * head), bf16),
             pltpu.VMEM((block_tokens, head), bf16),
             pltpu.VMEM((block_tokens, head), bf16),
@@ -905,17 +959,17 @@
             dma((sp_size,)),
             dma((tp_size,)),
             dma((tp_size,)),
-            dma((5, 19)),
-            dma((3, 3)),
-            dma((3, 2)),
-            dma((3, 2)),
-            dma((2, 6)),
-            dma((2, 3)),
+            dma((5, 17)),
+            dma((5, 3)),
+            dma((5, 2)),
+            dma((5, 2)),
+            dma((5, 6)),
+            dma((5, 3)),
             dma((5,)),
             dma((5,)),
             dma((5,)),
-            dma((5,)),
-            dma((5,)),
+            dma((2,)),
+            dma((2,)),
             dma((2,)),
             dma((2,)),
             dma((2 * chips,)),

time: 119 us -> 105 us (0.88)
  Pallas kernels: 116 us -> 102 us
    pallas_call x1, Pallas kernels: 116 us -> 102 us  [shards(): pl.pallas_call(functools.partial(kernel, sp_size, tp_size), out_shape=jax...]
where the time goes in v2:
time: 105 us
  Pallas kernels  102 us (97%)
  local copies, waits for them, and re-layouts  1.67 us (2%)
  between operations  1.31 us (1%)
    pallas_call x1, Pallas kernels, shards(): pl.pallas_call(functools.partial(kernel, sp_size, tp_size), out_shape=jax...  102 us

profile of v2, /device:TPU:1, one launch (start us, length us, event | category | flops | bytes accessed | tf_op | source)
XLA Modules:
  0.0 104.9 jit_solution(2864496383046790408)
XLA Ops:
  1.3 102.0 %layer.1 = bf16[32,4096]{1,0:T(8,128)(2,1)} custom-call(bf16[32,4096]{1,0:T(8,128)(2,1)} %latent.1, bf16[32,4096]{1,0:T(8,128)(2,1)} %context.1, f32[1,4096]{1,0:T(1,128)} %bitcast.3, f32[1,4096]{1,0:T(1,128)} %bitcast.4, bf16[3,256,256]{2,1,0:T(8,128)(2,1)} %modulation.1, bf16[4096,256]{1,0:T(8,128)(2,1)} %query_weight.1, bf16[4096,256]{1,0:T(8,128)(2,1)} %key_weight.1, ...), custom_call_target="tpu_custom_call" | custom-call | tf_op jit(solution)/shard_map/layer/pallas_call | solution.py:922
  103.3 1.7 %copy.20 = bf16[32,4096]{1,0:T(8,128)(2,1)} copy(bf16[32,4096]{1,0:T(8,128)(2,1)} %layer.1) | data formatting | bytes 524288

commit v3 on v2

--- a/solution.py
+++ b/solution.py
@@ -70,26 +70,19 @@
     ring_stage,
     from_left,
     from_right,
+    handed,
     local_sem,
     tok_send,
     tok_recv,
-    part_send,
-    part_recv,
-    piece_send,
-    piece_recv,
+    part_sem,
+    piece_sem,
     kv_send,
-    row_recv,
-    y_recv,
-    y2_recv,
-    col_recv,
-    x_recv,
+    stage_recv,
     dd_own,
     dd_ownb,
     dd_all,
-    q_send,
-    q_recv,
-    out_send,
-    out_recv,
+    q_sem,
+    out_sem,
     ps_sem,
     pr_sem,
     st_sem,
@@ -117,6 +110,9 @@
     def ring(v, n):
         return lax.rem(v + n, n)
 
+    def awaited(ref, sem):
+        pltpu.make_async_copy(ref, ref, sem).wait()
+
     def remote(src, dst, send_sem, recv_sem, sx, sy, sz, sc):
         return pltpu.make_async_remote_copy(
             src_ref=src,
@@ -194,7 +190,7 @@
         return remote(
             place,
             place,
-            tok_send.at[kind, 2 * b + part],
+            tok_send.at[0],
             tok_recv.at[2 * slot + part],
             x,
             y,
@@ -206,8 +202,8 @@
         return pltpu.make_async_remote_copy(
             src_ref=mod_parts.at[owner],
             dst_ref=mod_parts.at[owner],
-            send_sem=part_send.at[k],
-            recv_sem=part_recv.at[owner],
+            send_sem=part_sem.at[0],
+            recv_sem=part_sem.at[1],
             device_id={"sp": lax.rem(s + k, sp_size), "tp": t},
             device_id_type=MESH,
         )
@@ -216,8 +212,8 @@
         return pltpu.make_async_remote_copy(
             src_ref=mod_pieces.at[owner],
             dst_ref=mod_pieces.at[owner],
-            send_sem=piece_send.at[k],
-            recv_sem=piece_recv.at[owner],
+            send_sem=piece_sem.at[0],
+            recv_sem=piece_sem.at[1],
             device_id={"sp": s, "tp": lax.rem(t + k, tp_size)},
             device_id_type=MESH,
         )
@@ -229,8 +225,7 @@
     for part in range(2):
         token_copy(2, z, c, part).start()
 
-    for k in range(1, sp_size):
-        part_copy(k, lax.rem(s + k, sp_size)).wait_recv()
+    awaited(mod_parts.at[0 : sp_size - 1], part_sem.at[1])
     total = mod_parts[0]
     for i in range(1, sp_size):
         total = total + mod_parts[i]
@@ -256,8 +251,7 @@
         token_copy(2, right, c, left_part).start()
 
     forward(1, True)
-    for k in range(1, tp_size):
-        piece_copy(k, lax.rem(t + k, tp_size)).wait_recv()
+    awaited(mod_pieces.at[0 : tp_size - 1], piece_sem.at[1])
     for i in range(tp_size):
         mod_rows[:, i * piece : (i + 1) * piece] = mod_pieces[i]
 
@@ -271,7 +265,7 @@
 
     sizes = (ctx_rows + pair, 2 * pair, 2 * pair, 2 * pair, pair)
     starts = tuple(sum(sizes[:g]) for g in range(GROUPS))
-    firsts = (pair, pair, pair, pair, pair // 2)
+    firsts = (pair, pair, pair, pair, 3 * pair // 4)
     halves = tuple((firsts[g], sizes[g] - firsts[g]) for g in range(GROUPS))
     transit_starts = tuple(SIDE * sum(h[1] for h in halves[:g]) for g in range(GROUPS))
     own_kind = p == c
@@ -292,114 +286,88 @@
     def stage_at(g, q):
         return stage.at[aligned(starts[g] + q * halves[g][0], halves[g][q])]
 
-    def send(g, k, src, dst, recv_sem, sx, sy, sc):
-        return remote(src, dst, kv_send.at[g, k], recv_sem, sx, sy, z, sc)
-
-    def to_partner(g, k, ref, recv_sem=None):
-        return send(g, k, ref, ref, dd_all.at[g] if recv_sem is None else recv_sem, x, y, 1 - c)
-
-    def arrived(ref, recv_sem):
-        remote(ref, ref, kv_send.at[0, 0], recv_sem, x, y, z, 1 - c).wait_recv()
+    def send(step, src, dst, recv_sem, sx, sy, sc):
+        return remote(src, dst, kv_send.at[min(step - 1, 2)], recv_sem, sx, sy, z, sc)
+
+    def handed_at(g):
+        return handed.at[aligned(sum(h[0] for h in halves[:g]), halves[g][0])]
 
     def leaving(g, step, core=None):
         mine = []
+        here = stage_at(g, core) if step == 1 else None
 
         def add(cond, *args):
-            mine.append((cond, send(g, *args)))
-
-        def on(k, ref):
-            mine.append((None, to_partner(g, k, ref)))
+            mine.append((cond, send(step, *args)))
+
+        def on(ref):
+            add(None, ref, ref, dd_all.at[g], x, y, 1 - c)
+
+        def along_row(straight, aside, own, other):
+            there = kv_at(g, 0, x, y)
+            sem = stage_recv.at[g, 0]
+            add(other, aside, there, sem, xs[1], y, 0)
+            add(other, aside, there, sem, xs[3], y, 0)
+            add(own, straight, there, sem, xs[2], y, 0)
+
+        def along_column(straight, aside, own, other):
+            for cond, ref, there in ((own, straight, kv_at(g, 1, x, y)), (other, aside, transit_at(g, y))):
+                for k in (1, 3):
+                    add(cond, ref, there, stage_recv.at[g, 0], x, ys[k], 1)
 
         if step == 1:
-            for q, owner in ((0, 0), (1, 1)):
-                here = stage_at(g, q)
-                if q == 0:
-                    there = kv_at(g, 0, x, y)
-                    add(other_kind, 0, here, there, row_recv.at[g, 2], xs[1], y, owner)
-                    add(other_kind, 1, here, there, row_recv.at[g, 0], xs[3], y, owner)
-                    add(own_kind, 0, here, there, row_recv.at[g, 1], xs[2], y, owner)
-                    continue
-                for kind, cond, there in ((0, own_kind, kv_at(g, 1, x, y)), (1, other_kind, transit_at(g, y))):
-                    add(cond, 2, here, there, col_recv.at[g, 3 * kind], x, ys[1], owner)
-                    add(cond, 3, here, there, col_recv.at[g, 3 * kind + 1], x, ys[3], owner)
-            for q in range(2):
-                cond = own_kind & (c == q)
-                add(cond, 4, stage_at(g, 1 - q), kv_at(g, 1 - q, x, y), dd_own.at[g], x, y, 1 - c)
-                add(cond, 5, stage_at(g, q), kv_at(g, q, x, y), dd_ownb.at[g], x, y, 1 - c)
-            add(other_kind & (c == 0), 4, stage_at(g, 1), transit_at(g, y), dd_own.at[g], x, y, 1 - c)
+            there = kv_at(g, 1 - core, x, y)
+            far_half = stage_at(g, 1 - core)
+            add(own_kind, far_half, there, dd_own.at[g], x, y, 1 - c)
+            add(other_kind, far_half, handed_at(g) if core else transit_at(g, y), dd_own.at[g], x, y, 1 - c)
+            (along_column if core else along_row)(here, here, own_kind, other_kind)
+            add(own_kind, here, kv_at(g, core, x, y), dd_ownb.at[g], x, y, 1 - c)
         elif core == 0:
             if step == 2:
+                along_row(kv_at(g, 0, x, y), handed_at(g), other_kind, own_kind)
+            if step == 3:
                 line = kv_at(g, 0, 0, y, SIDE)
-                add(None, 6, line, line, y_recv.at[g, 0], x, ys[1], 0)
-                add(None, 7, line, line, y_recv.at[g, 1], x, ys[3], 0)
-                for k in range(3):
-                    on(8 + k, kv_at(g, 0, xs[k + 1], y))
-            if step == 3:
+                add(None, line, line, stage_recv.at[g, 1], x, ys[1], 0)
+                add(None, line, line, stage_recv.at[g, 1], x, ys[3], 0)
+                for k in (1, 2, 3):
+                    on(kv_at(g, 0, xs[k], y))
+            if step == 4:
                 low = kv_at(g, 0, 0, ys[3], 2)
                 high = kv_at(g, 0, 2, ys[1], 2)
-                add(None, 11, low, low, y2_recv.at[g, 0], x, ys[1], 0)
-                add(None, 12, high, high, y2_recv.at[g, 1], x, ys[3], 0)
-                on(13, kv_at(g, 0, 0, ys[3], SIDE))
-                on(14, kv_at(g, 0, 0, ys[1], SIDE))
-            if step == 4:
-                on(15, kv_at(g, 0, 0, ys[2], SIDE))
+                add(None, low, low, stage_recv.at[g, 2], x, ys[1], 0)
+                add(None, high, high, stage_recv.at[g, 2], x, ys[3], 0)
+                on(kv_at(g, 0, 0, ys[3], SIDE))
+                on(kv_at(g, 0, 0, ys[1], SIDE))
+            if step == 5:
+                on(kv_at(g, 0, 0, ys[2], SIDE))
         else:
             if step == 2:
+                along_column(kv_at(g, 1, x, y), transit_at(g, y), other_kind, own_kind)
+            if step == 3:
                 below = kv_at(g, 1, x, ys[3])
                 above = transit_at(g, ys[1])
-                add(None, 6, below, below, col_recv.at[g, 2], x, ys[1], 1)
-                add(None, 7, above, above, col_recv.at[g, 5], x, ys[3], 1)
-                on(8, below)
-                on(9, kv_at(g, 1, x, ys[1]))
-            if step == 3:
+                add(None, below, below, stage_recv.at[g, 1], x, ys[1], 1)
+                add(None, above, above, stage_recv.at[g, 1], x, ys[3], 1)
+                on(below)
+                on(kv_at(g, 1, x, ys[1]))
+            if step == 4:
                 line = kv_at(g, 1, x, 0, SIDE)
                 passing = transit_at(g, 0, SIDE)
-                add(None, 10, line, line, x_recv.at[g, 1], xs[2], y, 1)
-                add(None, 11, passing, line, x_recv.at[g, 2], xs[1], y, 1)
-                add(None, 12, passing, line, x_recv.at[g, 0], xs[3], y, 1)
-                on(13, kv_at(g, 1, x, ys[2]))
-            if step == 4:
-                for k in range(3):
-                    on(14 + k, kv_at(g, 1, xs[k + 1], 0, SIDE))
+                add(None, line, line, stage_recv.at[g, 2], xs[2], y, 1)
+                add(None, passing, line, stage_recv.at[g, 2], xs[1], y, 1)
+                add(None, passing, line, stage_recv.at[g, 2], xs[3], y, 1)
+                on(kv_at(g, 1, x, ys[2]))
+            if step == 5:
+                for k in (1, 2, 3):
+                    on(kv_at(g, 1, xs[k], 0, SIDE))
         return mine
 
     def arriving(g, step, core):
-        if core == 0:
-            if step == 2:
-                for k in range(3):
-                    arrived(kv_at(g, 0, xs[k + 1], y), row_recv.at[g, k])
-
-                @pl.when(other_kind)
-                def _():
-                    arrived(kv_at(g, 0, x, y), dd_own.at[g])
-
-            if step == 3:
-                arrived(kv_at(g, 0, 0, ys[3], SIDE), y_recv.at[g, 0])
-                arrived(kv_at(g, 0, 0, ys[1], SIDE), y_recv.at[g, 1])
-            if step == 4:
-                arrived(kv_at(g, 0, 0, ys[2], 2), y2_recv.at[g, 0])
-                arrived(kv_at(g, 0, 2, ys[2], 2), y2_recv.at[g, 1])
-            return
+        n = halves[g][core]
         if step == 2:
-            arrived(kv_at(g, 1, x, ys[3]), col_recv.at[g, 0])
-            arrived(transit_at(g, ys[1]), col_recv.at[g, 4])
-            arrived(kv_at(g, 1, x, ys[1]), col_recv.at[g, 1])
-            arrived(transit_at(g, ys[3]), col_recv.at[g, 3])
-        if step == 3:
-            arrived(kv_at(g, 1, x, ys[2]), col_recv.at[g, 2])
-            arrived(transit_at(g, ys[2]), col_recv.at[g, 5])
-
-            @pl.when(own_kind)
-            def _():
-                arrived(transit_at(g, y), dd_own.at[g])
-
-            @pl.when(other_kind)
-            def _():
-                arrived(kv_at(g, 1, x, y), dd_own.at[g])
-
-        if step == 4:
-            for k in range(3):
-                arrived(kv_at(g, 1, xs[k + 1], 0, SIDE), x_recv.at[g, k])
+            awaited(keys_values.at[0:n], dd_own.at[g])
+        else:
+            blocks = ((3, 8, 4), (4, 2, 12))[core][step - 3]
+            awaited(keys_values.at[0 : blocks * n], stage_recv.at[g, step - 3])
 
     def go(copies, wait=False):
         for cond, copy in copies:
@@ -421,19 +389,18 @@
 
             @pl.when(c == core)
             def _():
-                q = 1 - core
-                n = 15 * halves[g][q]
-                start = sp_size * (starts[g] + q * halves[g][0])
-                arrived(keys_values.at[start : start + n], dd_all.at[g])
+                n = halves[g][1 - core]
+                awaited(keys_values.at[0 : 15 * n], dd_all.at[g])
 
                 @pl.when(other_kind)
                 def _():
-                    arrived(kv_at(g, q, x, y), dd_ownb.at[g])
+                    awaited(keys_values.at[0:n], dd_ownb.at[g])
 
     def hand_out(g, keys, values):
         stage[starts[g] : starts[g] + sizes[g], :head] = keys
         stage[starts[g] : starts[g] + sizes[g], head:] = values
-        go(leaving(g, 1))
+        for core in range(2):
+            pl.when(c == core)(functools.partial(go, leaving(g, 1, core)))
         parts = (slice(0, halves[g][0]), slice(halves[g][0], sizes[g]))
 
         @pl.when(own_kind)
@@ -456,8 +423,8 @@
         return remote(
             q_stage.at[place],
             queries.at[place],
-            q_send.at[i],
-            q_recv.at[i],
+            q_sem.at[2],
+            q_sem.at[i],
             x + 1 - 2 * p,
             y,
             z,
@@ -536,6 +503,11 @@
         left = ring(z - d, chips)
         right = ring(z + d, chips)
 
+        @pl.when(d == 2)
+        def _():
+            relay(0, (0, 3))
+            relay(1, (0, 3))
+
         from_partner(left)
         from_partner(right)
         base = starts[1] + (d - 1) * 2 * pair
@@ -545,20 +517,20 @@
         @pl.when(d == 1)
         def _():
             forward(2, True)
-
-        @pl.when(d == 2)
-        def _():
-            forward(3, True)
             relay(0, (0, 2))
             relay(1, (0, 2))
+
+        @pl.when(d == 2)
+        def _():
+            forward(3, True)
 
         @pl.when(d == 3)
         def _():
             opposite = ring(z + far, chips)
             token_copy(2, opposite, c, 0).wait_recv()
             token_copy(2, opposite, c, 0).start()
-            relay(0, (1, 2))
-            relay(1, (1, 2), (0, 3))
+            relay(0, (0, 4))
+            relay(1, (1, 4))
 
         cos, sin = angles([left, right])
         v = normed[aligned(base, 2 * pair), :]
@@ -570,13 +542,23 @@
         @pl.when(d == 1)
         def _():
             forward(2, False)
+            relay(0, (1, 2))
+            relay(1, (1, 2))
+
+        @pl.when(d == 3)
+        def _():
+            relay(1, (2, 3))
 
         @pl.when(d == 2)
         def _():
+            relay(0, (1, 3))
+            relay(1, (1, 3), (0, 4))
             around = [z]
             for k in (1, 2):
                 around += [ring(z - k, chips), ring(z + k, chips)]
             ask(0, around)
+            relay(0, (2, 2))
+            relay(1, (2, 2))
             forward(3, False)
 
         return carry
@@ -586,30 +568,30 @@
     opposite = ring(z + far, chips)
     token_copy(2, opposite, c, 1).wait_recv()
     token_copy(2, opposite, c, 1).start()
-    relay(0, (2, 2))
+    relay(0, (3, 2))
+    relay(1, (3, 2))
     from_partner(opposite)
     normalise(tokens, opposite * pair, starts[4], pair, 0)
-    relay(1, (2, 2))
+    relay(0, (1, 4))
+    relay(1, (0, 5))
     cos, sin = angles([opposite])
     v = normed[starts[4] : starts[4] + pair, :]
     keys = turn(jnp.dot(v, wk[...], preferred_element_type=jnp.float32), cos, sin)
     values = jnp.dot(v, wv[...], preferred_element_type=jnp.float32).astype(jnp.bfloat16)
     hand_out(4, keys, values)
-    relay(0, (0, 3))
-    relay(1, (1, 3))
+    relay(0, (2, 3))
     ask(1, [ring(z - 3, chips), ring(z + 3, chips), opposite])
-    relay(0, (3, 2), (4, 2), (1, 3), (2, 3), (0, 4))
-    relay(1, (3, 2), (0, 4), (2, 3), (4, 2), (3, 3), (4, 3))
+    relay(0, (4, 2), (0, 5))
+    relay(1, (2, 4), (4, 2), (3, 3))
 
     peak[...] = jnp.full(peak.shape, -jnp.inf, jnp.float32)
     total_weight[...] = jnp.zeros(total_weight.shape, jnp.float32)
     mixed[...] = jnp.zeros(mixed.shape, jnp.float32)
 
-    @pl.when(other_kind)
-    def _():
-        for i in range(2):
-            place = queries.at[aligned(*q_parts[i])]
-            remote(place, place, q_send.at[i], q_recv.at[i], x, y, z, 1 - c).wait_recv()
+    def await_queries(i):
+        @pl.when(other_kind)
+        def _():
+            awaited(queries.at[aligned(*q_parts[i])], q_sem.at[i])
 
     my_head = 2 * z + p
     weight_of_second = mod_pieces[my_head, 6:7, 0:1]
@@ -647,15 +629,15 @@
         return remote(
             out_stage.at[first_row : first_row + n],
             attended.at[first_row : first_row + n],
-            out_send.at[i],
-            out_recv.at[i],
+            out_sem.at[3],
+            out_sem.at[i],
             x + 1 - 2 * p,
             y,
             z,
             1 - c,
         )
 
-    tiles = (q_parts[1], q_parts[0])
+    tiles = ((7 * pair, pair), (5 * pair, 2 * pair), q_parts[0])
 
     def finish(i):
         first_row, n = tiles[i]
@@ -681,6 +663,7 @@
     raised = jnp.where(on_context, lifted, 0.0)
     tile = block_tokens // 2
 
+    await_queries(0)
     complete(0)
 
     def first_group(i, carry):
@@ -688,13 +671,15 @@
 
         @pl.when(i == 0)
         def _():
-            relay(0, (3, 3))
+            await_queries(1)
+            relay(0, (1, 5))
+            relay(1, (1, 5), (4, 3))
 
         return carry
 
     lax.fori_loop(0, 2, first_group, 0)
-    relay(0, (4, 3), (1, 4))
-    relay(1, (1, 4))
+    relay(0, (2, 4), (3, 3))
+    relay(1, (3, 4))
     complete(1)
 
     def groups(j, carry):
@@ -704,42 +689,44 @@
 
         @pl.when(j == 0)
         def _():
-            relay(0, (2, 4))
-            relay(1, (2, 4))
+            relay(0, (4, 3))
+            relay(1, (4, 4))
 
         @pl.when(j == 1)
         def _():
+            relay(0, (2, 5))
+            relay(1, (2, 5))
             complete(2)
 
         @pl.when(j == 2)
         def _():
-            relay(0, (3, 4), (4, 4))
-            relay(1, (3, 4))
-
-        @pl.when(j == 3)
-        def _():
-            relay(1, (4, 4))
-            complete(3)
+            relay(0, (3, 4))
+            relay(1, (3, 5))
 
         return carry
 
-    lax.fori_loop(0, 6, groups, 0)
+    lax.fori_loop(0, 4, groups, 0)
+    relay(0, (4, 4), (3, 5))
+    complete(3)
+    locals_[6].wait()
+    base = sp_size * starts[3]
+    count = sp_size * sizes[3]
+    rest = sp_size * sizes[4]
+    attend(base, count, *q_parts[1])
+    relay(0, (4, 5))
+    relay(1, (4, 5))
     complete(4)
-    locals_[6].wait()
-
-    def last_group(i):
-        attend(sp_size * starts[4], sp_size * sizes[4], tiles[i][0], tiles[i][1])
+    for i in range(2):
+        attend(base + count, rest, *tiles[i])
         finish(i)
-
-    last_group(0)
-    last_group(1)
+    attend(base, count, *tiles[2])
 
     span = width // 2
     chunk = 1024
 
     def pair_copy(u):
         ref = pair_send.at[u]
-        return remote(ref, pair_recv.at[u], ps_sem.at[u], pr_sem.at[u], x, y, z, 1 - c)
+        return remote(ref, pair_recv.at[u], ps_sem.at[0], pr_sem.at[u], x, y, z, 1 - c)
 
     def ring_copy(side, d, part):
         u = 2 * d + part
@@ -748,14 +735,14 @@
         to = (ring(z + 1, chips), ring(z - 1, chips))[side]
         v = 2 * (d - 1) + part
         return remote(
-            ring_stage.at[side, u], into.at[v], st_sem.at[side, u], sem.at[v], x, y, to, c
+            ring_stage.at[side, u], into.at[v], st_sem.at[side], sem.at[v], x, y, to, c
         )
 
     def ring_arrived(side, d, part):
         v = 2 * d + part
         into = (from_left, from_right)[side]
         sem = (left_sem, right_sem)[side]
-        remote(into.at[v], into.at[v], st_sem.at[side, v], sem.at[v], x, y, z, 1 - c).wait_recv()
+        awaited(into.at[v], sem.at[v])
 
     def block_of(side, d):
         if d == 0:
@@ -794,63 +781,58 @@
         ring_stage[side, 2 * d + part] = value.astype(jnp.bfloat16)
         ring_copy(side, d, part).start()
 
-    @pl.when(other_kind)
-    def _():
-        first_row, n = tiles[0]
-        out_copy(0, first_row, n).wait_recv()
-
+    def await_attended(i):
+        @pl.when(other_kind)
+        def _():
+            awaited(attended.at[aligned(*tiles[i])], out_sem.at[i])
+
+    await_attended(0)
     compute(4)
     combine(0, 4, 0)
     combine(1, 4, 1)
+    await_attended(1)
     compute(3)
     combine(0, 3, 1)
     combine(1, 3, 0)
+    attend(base + count, rest, *tiles[2])
+    finish(2)
     combine(0, 3, 0)
     combine(1, 3, 1)
 
-    @pl.when(other_kind)
-    def _():
-        first_row, n = tiles[1]
-        out_copy(1, first_row, n).wait_recv()
-
+    await_attended(2)
     compute(2)
     combine(0, 2, 1)
     combine(1, 2, 0)
     compute(1)
 
-    for part in range(2):
-        for d in range(far):
-            if d < far - 1 or part == 0:
-                token_copy(0, ring(z - d, chips), c, part).wait_send()
-            if d < far - 1 or part == 1:
-                token_copy(1, ring(z + d, chips), c, part).wait_send()
-        for b in range(chips):
-            token_copy(2, b, c, part).wait_send()
-    for k in range(1, tp_size):
-        piece_copy(k, t).wait_send()
-    for k in range(1, sp_size):
-        part_copy(k, s).wait_send()
+    awaited(tokens.at[0 : 2 * (2 * far - 1) * part_rows + block_tokens // 2], tok_send.at[0])
+    awaited(mod_parts.at[0 : sp_size - 1], part_sem.at[0])
+    awaited(mod_pieces.at[0 : tp_size - 1], piece_sem.at[0])
     combine(0, 2, 0)
     combine(1, 2, 1)
     compute(0)
-    for g in range(GROUPS):
-        go(leaving(g, 1), True)
+    first_rows = sum(h[0] for h in halves)
+    second_rows = sum(h[1] for h in halves)
     for core in range(2):
-
-        @pl.when(c == core)
-        def _():
-            for g in range(GROUPS):
-                for step in (2, 3, 4):
-                    go(leaving(g, step, core), True)
+        for cond, kind in ((own_kind, 0), (other_kind, 1)):
+
+            @pl.when((c == core) & cond)
+            def _():
+                alone = (first_rows, second_rows)[core]
+                away = (first_rows, second_rows)[1 - core]
+                own_sends, later = ((2, 27), (3, 29))[core]
+                once = away + (own_sends if kind == 0 else 2) * alone
+                handed_on = (1 if core == 0 and kind == 1 else 2) * alone
+                awaited(keys_values.at[0:once], kv_send.at[0])
+                awaited(keys_values.at[0:handed_on], kv_send.at[1])
+                awaited(keys_values.at[0 : later * alone], kv_send.at[2])
 
     @pl.when(other_kind)
     def _():
-        for i in range(2):
-            q_copy(i).wait_send()
-            out_copy(i, tiles[i][0], tiles[i][1]).wait_send()
-
-    for u in range(2 * chips):
-        pair_copy(u).wait_send()
+        awaited(queries, q_sem.at[2])
+        awaited(attended, out_sem.at[3])
+
+    awaited(pair_send, ps_sem.at[0])
     combine(0, 1, 1)
     combine(1, 1, 0)
     combine(0, 1, 0)
@@ -869,10 +851,7 @@
         ).astype(jnp.bfloat16)
 
     for side in range(2):
-        ring_copy(side, far, side).wait_send()
-        for d in (1, 2, 3):
-            for part in range(2):
-                ring_copy(side, d, part).wait_send()
+        awaited(ring_stage.at[side, 0 : 2 * far - 1], st_sem.at[side])
 
 
 def tables(half):
@@ -952,29 +931,22 @@
             pltpu.VMEM((2, chips + 2, rows, width // 2), bf16),
             pltpu.VMEM((chips, rows, width // 2), bf16),
             pltpu.VMEM((chips, rows, width // 2), bf16),
+            pltpu.VMEM((5 * pair, 2 * head), bf16),
             dma((7,)),
-            dma((3, 2 * chips)),
+            dma((1,)),
             dma((2 * tp_size,)),
-            dma((sp_size,)),
-            dma((sp_size,)),
-            dma((tp_size,)),
-            dma((tp_size,)),
-            dma((5, 17)),
-            dma((5, 3)),
-            dma((5, 2)),
-            dma((5, 2)),
-            dma((5, 6)),
+            dma((2,)),
+            dma((2,)),
+            dma((3,)),
             dma((5, 3)),
             dma((5,)),
             dma((5,)),
             dma((5,)),
+            dma((3,)),
+            dma((4,)),
+            dma((1,)),
+            dma((2 * chips,)),
             dma((2,)),
-            dma((2,)),
-            dma((2,)),
-            dma((2,)),
-            dma((2 * chips,)),
-            dma((2 * chips,)),
-            dma((2, chips + 2)),
             dma((chips,)),
             dma((chips,)),
         ],

time: 105 us -> 99.7 us (0.950)
  Pallas kernels: 102 us -> 96.5 us
    pallas_call x1, Pallas kernels: 102 us -> 96.5 us  [shards(): pl.pallas_call(functools.partial(kernel, sp_size, tp_size), out_shape=jax...]
where the time goes in v3:
time: 99.7 us; the launch traced here: 99.5 us
  Pallas kernels  96.5 us (97%)
  local copies, waits for them, and re-layouts  1.67 us (2%)
  between operations  1.31 us (1%)
    pallas_call x1, Pallas kernels, shards(): pl.pallas_call(functools.partial(kernel, sp_size, tp_size), out_shape=jax...  96.5 us

profile of v3, /device:TPU:1, one launch (start us, length us, event | category | flops | bytes accessed | tf_op | source)
XLA Modules:
  0.0 99.5 jit_solution(11013037060860244298)
XLA Ops:
  1.3 96.5 %layer.1 = bf16[32,4096]{1,0:T(8,128)(2,1)} custom-call(bf16[32,4096]{1,0:T(8,128)(2,1)} %latent.1, bf16[32,4096]{1,0:T(8,128)(2,1)} %context.1, f32[1,4096]{1,0:T(1,128)} %bitcast.3, f32[1,4096]{1,0:T(1,128)} %bitcast.4, bf16[3,256,256]{2,1,0:T(8,128)(2,1)} %modulation.1, bf16[4096,256]{1,0:T(8,128)(2,1)} %query_weight.1, bf16[4096,256]{1,0:T(8,128)(2,1)} %key_weight.1, ...), custom_call_target="tpu_custom_call" | custom-call | tf_op jit(solution)/shard_map/layer/pallas_call | solution.py:901
  97.9 1.7 %copy.20 = bf16[32,4096]{1,0:T(8,128)(2,1)} copy(bf16[32,4096]{1,0:T(8,128)(2,1)} %layer.1) | data formatting | bytes 524288

commit v4 on v3

--- a/solution.py
+++ b/solution.py
@@ -498,18 +498,24 @@
     values = jnp.dot(normed[: sizes[0], :], wv[...], preferred_element_type=jnp.float32).astype(jnp.bfloat16)
     hand_out(0, keys, values)
     forward(1, False)
+    relay(0, (0, 2))
+    relay(1, (0, 2))
 
     def process(d, carry):
         left = ring(z - d, chips)
         right = ring(z + d, chips)
 
-        @pl.when(d == 2)
-        def _():
-            relay(0, (0, 3))
-            relay(1, (0, 3))
-
         from_partner(left)
         from_partner(right)
+
+        @pl.when(d == 2)
+        def _():
+            relay(1, (0, 4))
+
+        @pl.when(d == 3)
+        def _():
+            relay(1, (1, 4))
+
         base = starts[1] + (d - 1) * 2 * pair
         normalise(tokens, left * pair, base, pair, 0)
         normalise(tokens, right * pair, base + pair, pair, 0)
@@ -517,8 +523,6 @@
         @pl.when(d == 1)
         def _():
             forward(2, True)
-            relay(0, (0, 2))
-            relay(1, (0, 2))
 
         @pl.when(d == 2)
         def _():
@@ -529,8 +533,6 @@
             opposite = ring(z + far, chips)
             token_copy(2, opposite, c, 0).wait_recv()
             token_copy(2, opposite, c, 0).start()
-            relay(0, (0, 4))
-            relay(1, (1, 4))
 
         cos, sin = angles([left, right])
         v = normed[aligned(base, 2 * pair), :]
@@ -541,6 +543,8 @@
 
         @pl.when(d == 1)
         def _():
+            relay(0, (0, 3))
+            relay(1, (0, 3))
             forward(2, False)
             relay(0, (1, 2))
             relay(1, (1, 2))
@@ -552,12 +556,12 @@
         @pl.when(d == 2)
         def _():
             relay(0, (1, 3))
-            relay(1, (1, 3), (0, 4))
+            relay(1, (1, 3))
             around = [z]
             for k in (1, 2):
                 around += [ring(z - k, chips), ring(z + k, chips)]
             ask(0, around)
-            relay(0, (2, 2))
+            relay(0, (0, 4), (2, 2))
             relay(1, (2, 2))
             forward(3, False)
 
@@ -672,13 +676,13 @@
         @pl.when(i == 0)
         def _():
             await_queries(1)
-            relay(0, (1, 5))
+            relay(0, (3, 3), (1, 5))
             relay(1, (1, 5), (4, 3))
 
         return carry
 
     lax.fori_loop(0, 2, first_group, 0)
-    relay(0, (2, 4), (3, 3))
+    relay(0, (2, 4), (4, 3))
     relay(1, (3, 4))
     complete(1)
 
@@ -689,32 +693,31 @@
 
         @pl.when(j == 0)
         def _():
-            relay(0, (4, 3))
+            relay(0, (3, 4))
             relay(1, (4, 4))
 
         @pl.when(j == 1)
         def _():
-            relay(0, (2, 5))
+            relay(0, (2, 5), (4, 4))
             relay(1, (2, 5))
             complete(2)
 
         @pl.when(j == 2)
         def _():
-            relay(0, (3, 4))
+            relay(0, (3, 5))
             relay(1, (3, 5))
 
         return carry
 
     lax.fori_loop(0, 4, groups, 0)
-    relay(0, (4, 4), (3, 5))
+    relay(0, (4, 5))
+    relay(1, (4, 5))
     complete(3)
     locals_[6].wait()
     base = sp_size * starts[3]
     count = sp_size * sizes[3]
     rest = sp_size * sizes[4]
     attend(base, count, *q_parts[1])
-    relay(0, (4, 5))
-    relay(1, (4, 5))
     complete(4)
     for i in range(2):
         attend(base + count, rest, *tiles[i])

time: 99.7 us -> 96.8 us (0.971)
  Pallas kernels: 96.5 us -> 93 us
    pallas_call x1, Pallas kernels: 96.5 us -> 93 us  [shards(): pl.pallas_call(functools.partial(kernel, sp_size, tp_size), out_shape=jax...]
where the time goes in v4:
time: 96.8 us; the launch traced here: 96 us
  Pallas kernels  93 us (96%)
  local copies, waits for them, and re-layouts  1.67 us (2%)
  between operations  1.31 us (1%)
    pallas_call x1, Pallas kernels, shards(): pl.pallas_call(functools.partial(kernel, sp_size, tp_size), out_shape=jax...  93 us

profile of v4, /device:TPU:1, one launch (start us, length us, event | category | flops | bytes accessed | tf_op | source)
XLA Modules:
  0.0 96.0 jit_solution(3316999473134667964)
XLA Ops:
  1.3 93.0 %layer.1 = bf16[32,4096]{1,0:T(8,128)(2,1)} custom-call(bf16[32,4096]{1,0:T(8,128)(2,1)} %latent.1, bf16[32,4096]{1,0:T(8,128)(2,1)} %context.1, f32[1,4096]{1,0:T(1,128)} %bitcast.3, f32[1,4096]{1,0:T(1,128)} %bitcast.4, bf16[3,256,256]{2,1,0:T(8,128)(2,1)} %modulation.1, bf16[4096,256]{1,0:T(8,128)(2,1)} %query_weight.1, bf16[4096,256]{1,0:T(8,128)(2,1)} %key_weight.1, ...), custom_call_target="tpu_custom_call" | custom-call | tf_op jit(solution)/shard_map/layer/pallas_call | solution.py:904
  94.3 1.7 %copy.20 = bf16[32,4096]{1,0:T(8,128)(2,1)} copy(bf16[32,4096]{1,0:T(8,128)(2,1)} %layer.1) | data formatting | bytes 524288
